TPU v7x, 32 devices: a whole 2x2x4 slice. The times are simulated.
32 devices in a mesh: grp: 2 (over y), fs: 4 (over z), tp: 4 (over x, core).
Axes of the slice: x: 2, y: 2, z: 4, core: 2. Of those that a mesh axis runs over, the one named last changes fastest.
Arguments:
- tokens: bfloat16 [1536, 2048], P(('grp', 'tp')), parts along dimension 0, may hold values from -6 to 6
- norm_gain: float32 [2048], P('fs'), may hold values from 0.1 to 1.9
- up_trained: float32 [2048, 8192], P('fs', 'tp'), may hold values from -0.125 to 0.125
- down_trained: float32 [2048, 8192], P('fs', 'tp'), may hold values from -0.09375 to 0.09375
Outputs:
- up_serving: bfloat16 [4096, 8192], P('grp', 'fs'), parts along dimension 0
- down_serving: bfloat16 [4096, 8192], P('grp', 'fs'), parts along dimension 0
- prompt_output: bfloat16 [1536, 2048], P(('grp', 'tp'), 'fs'), parts along dimension 0
There are 2 independent parts, one for each index of `grp`. A program takes and returns all parts, laid end to end along the dimension named above; an argument that names none is the same for every part. Nothing has to cross between parts.
All inputs are finite; a program needn't handle non-finite values.
Results may differ from a plain program's by a relative error of at most 0.0074.
Values may be sent and summed in bfloat16 or wider, within the bound.
A program may use at most 128 MiB of HBM per device.

v0:
```python
import functools

import jax
import jax.numpy as jnp
from jax import lax
from jax.experimental import pallas as pl
from jax.experimental.pallas import tpu as pltpu
from jax.sharding import PartitionSpec as P

epsilon = 1e-06
MESH = pl.DeviceIdType.MESH


def local_plain(tokens, norm_gain, up_trained, down_trained):
    shards = lax.axis_size("fs")
    groups = lax.axis_size("tp")
    rows_local = up_trained.shape[0]
    cols_local = up_trained.shape[1]
    folded = (norm_gain[:, None] * up_trained).astype(jnp.bfloat16)
    stacked = jnp.stack([folded, down_trained.astype(jnp.bfloat16)])
    served_width = cols_local * groups // shards
    blocks_here = cols_local // served_width
    quarter_rows = rows_local // groups
    pieces = stacked.reshape(2, groups, quarter_rows, blocks_here, served_width)
    moved = lax.all_to_all(pieces, "tp", split_axis=1, concat_axis=3, tiled=True)
    placed = lax.all_to_all(moved, "fs", split_axis=3, concat_axis=2, tiled=True)
    ordered = placed.reshape(2, shards, quarter_rows, served_width)
    joined = lax.all_gather(ordered, "tp", axis=2, tiled=True)
    owned = joined.reshape(2, rows_local * shards, served_width)
    up_serving = owned[0]
    down_serving = owned[1]
    values = tokens.astype(jnp.float32)
    scale = lax.rsqrt(jnp.mean(values * values, axis=1, keepdims=True) + epsilon)
    normed = (values * scale).astype(jnp.bfloat16)
    hidden = jnp.dot(normed, up_serving, preferred_element_type=jnp.float32)
    active = jnp.square(jax.nn.relu(hidden)).astype(jnp.bfloat16)
    summed = lax.psum_scatter(
        lax.dot_general(
            down_serving, active, (((1,), (1,)), ((), ())), preferred_element_type=jnp.float32
        ),
        "fs",
        scatter_dimension=0,
        tiled=True,
    )
    prompt_output = summed.T.astype(jnp.bfloat16)
    return (up_serving, down_serving, prompt_output)


def xor2(a, k):
    if k % 2:
        a = a + 1 - 2 * (a % 2)
    if k // 2:
        a = a + 2 - 4 * (a // 2)
    return a


def kernel(
    tokens_hbm, gain_hbm, up_hbm, down_hbm, whole, prompt_out,
    raw, gain, cast, swapped, toks, normed, hidden, active, rs_send, rs_recv, rs_own,
    in_sem, misc_sem, own_sem,
    x1_send, x1_recv, z_send, z_recv,
    ax_send, ax_recv, ay_send, ay_recv, dg_send, dg_recv, d2_send, d2_recv,
    rs_ssem, rs_rsem,
):
    y = lax.axis_index("grp")
    z = lax.axis_index("fs")
    t = lax.axis_index("tp")
    x, c = t // 2, t % 2
    t_x = xor2(t, 2)
    t_c = xor2(t, 1)
    to_x = {"tp": t_x}
    to_c = {"tp": t_c}
    to_y = {"grp": 1 - y}
    quarter, width = cast.shape[2], cast.shape[3]
    rows_local = 4 * quarter
    trained = (up_hbm, down_hbm)

    def part_rows(px, py):
        return pl.multiple_of((2 * px + py) * quarter, quarter)

    fetch = {}
    for m in range(2):
        for s, px in ((0, 1 - x), (1, x)):
            fetch[m, s] = pltpu.make_async_copy(
                trained[m].at[pl.ds(part_rows(px, y), quarter)], raw.at[m, s], in_sem.at[m, s]
            )
    get_gain = pltpu.make_async_copy(gain_hbm, gain, misc_sem.at[0])
    get_toks = pltpu.make_async_copy(tokens_hbm, toks, misc_sem.at[1])
    get_gain.start()
    for m in range(2):
        for s in range(2):
            fetch[m, s].start()
    get_toks.start()

    barrier = pltpu.get_barrier_semaphore()
    for where in (to_x, to_c, to_y, {"fs": xor2(z, 1)}, {"fs": xor2(z, 2)}, {"fs": xor2(z, 3)}):
        pl.semaphore_signal(barrier, inc=1, device_id=where, device_id_type=MESH)
    pl.semaphore_wait(barrier, 6)

    def remote(src, dst, ssem, rsem, where):
        return pltpu.make_async_remote_copy(
            src_ref=src, dst_ref=dst, send_sem=ssem, recv_sem=rsem,
            device_id=where, device_id_type=MESH,
        )

    def unit(m, r, px, py):
        start = pl.multiple_of(r * rows_local + (2 * px + py) * quarter, quarter)
        return whole.at[m, pl.ds(start, quarter)]

    def hop(m, j):
        block = (t, t_x)[j]
        src = (cast.at[m, 1], swapped.at[m])[j]
        k = (z + block) % 2 + 2 * ((z // 2 + block // 2) % 2)
        return remote(
            src, unit(m, z, x, y), z_send.at[m, j], z_recv.at[m, k], {"fs": block}
        )

    def own_copy(m, j):
        src = (cast.at[m, 1], swapped.at[m])[j]
        return pltpu.make_async_copy(src, unit(m, z, x, y), own_sem.at[m])

    def start_hop(m, j):
        block = (t, t_x)[j]

        @pl.when(z != block)
        def _():
            hop(m, j).start()

        @pl.when(z == block)
        def _():
            own_copy(m, j).start()

    swap = {
        m: remote(cast.at[m, 0], swapped.at[m], x1_send.at[m], x1_recv.at[m], to_x)
        for m in range(2)
    }

    piece = 16

    def cast_part(m, s):
        px = 1 - x if s == 0 else x
        base = part_rows(px, y)
        fetch[m, s].wait()

        @pl.loop(0, quarter // piece)
        def _(i):
            here = pl.ds(pl.multiple_of(i * piece, piece), piece)
            values = raw[m, s, here, :]
            if m == 0:
                values = values * gain[pl.ds(pl.multiple_of(base + i * piece, piece), piece), :]
            cast[m, s, here, :] = values.astype(jnp.bfloat16)

    get_gain.wait()
    cast_part(0, 0)
    swap[0].start()
    cast_part(0, 1)
    start_hop(0, 0)
    cast_part(1, 0)
    swap[1].start()
    cast_part(1, 1)
    start_hop(1, 0)

    get_toks.wait()
    tokens_here = toks.shape[0]

    @pl.loop(0, tokens_here // piece)
    def _(i):
        here = pl.ds(pl.multiple_of(i * piece, piece), piece)
        values = toks[here, :].astype(jnp.float32)
        scale = lax.rsqrt(jnp.mean(values * values, axis=1, keepdims=True) + epsilon)
        normed[here, :] = (values * scale).astype(jnp.bfloat16)

    swap[0].wait_recv()
    start_hop(0, 1)

    steps = [(m, k) for m in range(2) for k in range(4)]
    diag_by_x = {(0, 0), (1, 0), (0, 2), (1, 2)}

    def copies(m, k):
        r = xor2(z, k)
        mine = unit(m, r, x, y)
        from_x = unit(m, r, 1 - x, y)
        from_y = unit(m, r, x, 1 - y)
        diag = unit(m, r, 1 - x, 1 - y)
        made = {
            "x": remote(mine, mine, ax_send.at[m, k], ax_recv.at[m, k], to_x),
            "y": remote(mine, mine, ay_send.at[m, k], ay_recv.at[m, k], to_y),
        }
        if (m, k) in diag_by_x:
            made["diag"] = remote(from_y, from_y, dg_send.at[m, k], dg_recv.at[m, k], to_x)
        else:
            made["diag"] = remote(from_x, from_x, dg_send.at[m, k], dg_recv.at[m, k], to_y)
        for p, ref in enumerate((mine, from_x, from_y, diag)):
            made[p] = remote(ref, ref, d2_send.at[m, k, p], d2_recv.at[m, k, p], to_c)
        return made

    is_active = c == z % 2
    lag_b, lag_c = 1, 2

    def stage_a(m, k):
        made = copies(m, k)
        if k == 0:
            own_copy(m, 0).wait()
        else:
            here = unit(m, xor2(z, k), x, y)
            remote(here, here, z_send.at[m, 0], z_recv.at[m, k], {"fs": xor2(z, k)}).wait_recv()
        made["x"].start()
        made["y"].start()
        made[0].start()

    def stage_b(m, k):
        made = copies(m, k)
        made["x"].wait_recv()
        if (m, k) not in diag_by_x:
            made["diag"].start()
        made[1].start()
        made["y"].wait_recv()
        if (m, k) in diag_by_x:
            made["diag"].start()
        made[2].start()

    def stage_c(m, k):
        made = copies(m, k)
        made["diag"].wait_recv()
        made[3].start()

    def listen(m, k):
        made = copies(m, k)
        for p in range(4):
            made[p].wait_recv()

    tile = 512 if width % 512 == 0 else width

    def compute_up(k):
        r = xor2(z, k)
        rows = pl.ds(pl.multiple_of(r * rows_local, rows_local), rows_local)
        left = normed[:, rows]

        @pl.loop(0, width // tile)
        def _(n):
            cols = pl.ds(pl.multiple_of(n * tile, tile), tile)
            product = jnp.dot(left, whole[0, rows, cols], preferred_element_type=jnp.float32)
            if k > 0:
                product = product + hidden[:, cols]
            if k < 3:
                hidden[:, cols] = product
            else:
                active[:, cols] = jnp.square(jnp.maximum(product, 0.0)).astype(jnp.bfloat16)

    d_tile = 256 if rows_local % 256 == 0 else rows_local

    def compute_down(k):
        r = xor2(z, k)

        @pl.loop(0, rows_local // d_tile)
        def _(n):
            cols = pl.ds(pl.multiple_of(n * d_tile, d_tile), d_tile)
            rows = pl.ds(pl.multiple_of(r * rows_local + n * d_tile, d_tile), d_tile)
            product = lax.dot_general(
                active[...], whole[1, rows, :], (((1,), (1,)), ((), ())),
                preferred_element_type=jnp.float32,
            )
            if k > 0:
                rs_send[k - 1, :, cols] = product.astype(jnp.bfloat16)
            else:
                rs_own[:, cols] = product

    def scatter(k):
        return remote(
            rs_send.at[k - 1], rs_recv.at[k - 1], rs_ssem.at[k - 1], rs_rsem.at[k - 1],
            {"fs": xor2(z, k)},
        )

    for i in range(len(steps) + lag_c):
        @pl.when(is_active)
        def _():
            if i < len(steps):
                stage_a(*steps[i])
            if 0 <= i - lag_b < len(steps):
                stage_b(*steps[i - lag_b])
            if 0 <= i - lag_c < len(steps):
                stage_c(*steps[i - lag_c])

        if i == 1:
            swap[1].wait_recv()
            start_hop(1, 1)
        if i < lag_c:
            continue
        m, k = steps[i - lag_c]

        @pl.when(jnp.logical_not(is_active))
        def _():
            listen(m, k)

        if m == 0:
            compute_up(k)
        elif k > 0:
            compute_down(k)
            scatter(k).start()

    compute_down(0)
    for k in range(1, 4):
        scatter(k).wait_recv()

    @pl.loop(0, tokens_here // piece)
    def _(i):
        here = pl.ds(pl.multiple_of(i * piece, piece), piece)
        total = rs_own[here, :]
        for k in range(3):
            total = total + rs_recv[k, here, :].astype(jnp.float32)
        prompt_out[here, :] = total.astype(prompt_out.dtype)

    for m in range(2):
        swap[m].wait_send()
        for j in range(2):
            block = (t, t_x)[j]

            @pl.when(z != block)
            def _():
                hop(m, j).wait_send()
    for k in range(1, 4):
        scatter(k).wait_send()

    @pl.when(is_active)
    def _():
        for m, k in steps:
            made = copies(m, k)
            for copy in made.values():
                copy.wait_send()


pieces_out = 8


def deliver(whole, prompt, up_out, down_out, prompt_out, sems, last):
    rows = whole.shape[1] // pieces_out
    copies = [
        pltpu.make_async_copy(
            whole.at[m, pl.ds(i * rows, rows)], out.at[pl.ds(i * rows, rows)], sems.at[m, i]
        )
        for m, out in enumerate((up_out, down_out))
        for i in range(pieces_out)
    ]
    copies.append(pltpu.make_async_copy(prompt, prompt_out, last))
    for copy in copies:
        copy.start()
    for copy in copies:
        copy.wait()


def local_kernel(tokens, norm_gain, up_trained, down_trained):
    shards = lax.axis_size("fs")
    rows_local, width = up_trained.shape
    quarter = rows_local // 4
    tokens_here, features = tokens.shape
    any_space = pl.BlockSpec(memory_space=pl.ANY)
    dma = pltpu.SemaphoreType.DMA
    bf16, f32 = jnp.bfloat16, jnp.float32
    whole, prompt = pl.pallas_call(
        kernel,
        out_shape=(
            pltpu.VMEM((2, rows_local * shards, width), bf16),
            pltpu.VMEM((tokens_here, rows_local), bf16),
        ),
        in_specs=[any_space] * 4,
        out_specs=(pl.BlockSpec(memory_space=pltpu.VMEM),) * 2,
        scratch_shapes=[
            pltpu.VMEM((2, 2, quarter, width), f32),
            pltpu.VMEM((rows_local, 1), f32),
            pltpu.VMEM((2, 2, quarter, width), bf16),
            pltpu.VMEM((2, quarter, width), bf16),
            pltpu.VMEM((tokens_here, features), bf16),
            pltpu.VMEM((tokens_here, features), bf16),
            pltpu.VMEM((tokens_here, width), f32),
            pltpu.VMEM((tokens_here, width), bf16),
            pltpu.VMEM((3, tokens_here, rows_local), bf16),
            pltpu.VMEM((3, tokens_here, rows_local), bf16),
            pltpu.VMEM((tokens_here, rows_local), f32),
            dma((2, 2)), dma((2,)), dma((2,)),
            dma((2,)), dma((2,)), dma((2, 2)), dma((2, 4)),
            dma((2, 4)), dma((2, 4)), dma((2, 4)), dma((2, 4)),
            dma((2, 4)), dma((2, 4)), dma((2, 4, 4)), dma((2, 4, 4)),
            dma((3,)), dma((3,)),
        ],
        compiler_params=pltpu.CompilerParams(
            collective_id=0, has_side_effects=True, vmem_limit_bytes=40 * 1024 * 1024
        ),
    )(tokens, norm_gain[:, None], up_trained, down_trained)
    held = pl.BlockSpec(memory_space=pltpu.VMEM)
    return tuple(pl.pallas_call(
        deliver,
        out_shape=(
            jax.ShapeDtypeStruct((rows_local * shards, width), bf16),
            jax.ShapeDtypeStruct((rows_local * shards, width), bf16),
            jax.ShapeDtypeStruct((tokens_here, rows_local), bf16),
        ),
        in_specs=[held, held],
        out_specs=(any_space,) * 3,
        scratch_shapes=[dma((2, pieces_out)), dma(())],
        compiler_params=pltpu.CompilerParams(vmem_limit_bytes=8 * 1024 * 1024),
    )(whole, prompt))


def solution(mesh):
    in_specs = (P(("grp", "tp"), None), P("fs"), P("fs", "tp"), P("fs", "tp"))
    out_specs = (P("grp", "fs"), P("grp", "fs"), P(("grp", "tp"), "fs"))
    sizes = mesh.shape
    square = sizes["grp"] == 2 and sizes["fs"] == 4 and sizes["tp"] == 4
    local = local_kernel if square else local_plain
    return jax.shard_map(local, mesh=mesh, in_specs=in_specs, out_specs=out_specs, check_vma=False)
```

profile of v0, /device:TPU:3, one launch (start us, length us, event | category | flops | bytes accessed | tf_op | source)
XLA Modules:
  0.0 128.0 jit_solution(4337218767772625601)
XLA Ops:
  0.6 1.5 %copy.7.gain_hbm = f32[512,1]{1,0:T(8,128)} copy(f32[512,1]{0,1:T(1,128)} %bitcast.1) | data formatting | bytes 4096 | tf_op jit(solution)/shard_map/broadcast_in_dim | solution.py:388
  2.2 119.9 %shard_map.67 = (bf16[2,2048,2048]{2,1,0:T(8,128)(2,1)S(1)}, bf16[192,512]{1,0:T(8,128)(2,1)S(1)}) custom-call(bf16[192,2048]{1,0:T(8,128)(2,1)} %tokens_hbm.1, f32[512,1]{1,0:T(8,128)} %copy.7.gain_hbm, f32[512,2048]{1,0:T(8,128)} %up_hbm.1, f32[512,2048]{1,0:T(8,128)} %down_hbm.1), custom_call_target="tpu_custom_call" | custom-call | tf_op jit(solution)/shard_map/pallas_call | solution.py:359
  122.0 6.0 %shard_map.68 = (bf16[2048,2048]{1,0:T(8,128)(2,1)}, bf16[2048,2048]{1,0:T(8,128)(2,1)}, bf16[192,512]{1,0:T(8,128)(2,1)}) custom-call(bf16[2,2048,2048]{2,1,0:T(8,128)(2,1)S(1)} %get-tuple-element.5.whole, bf16[192,512]{1,0:T(8,128)(2,1)S(1)} %get-tuple-element.6.prompt), custom_call_target="tpu_custom_call" | custom-call | tf_op jit(solution)/shard_map/pallas_call | solution.py:390
where the time goes:
time: 129 us; the launch traced here: 128 us
  Pallas kernels  126 us (98%)
  local copies, waits for them, and re-layouts  1.53 us (1%)
    pallas_call x1, Pallas kernels, local_kernel(): pl.pallas_call(kernel, out_shape=(pltpu.VMEM((2, rows_local * shards, wid...  120 us
    pallas_call x1, Pallas kernels, local_kernel(): pl.pallas_call(deliver, out_shape=(jax.ShapeDtypeStruct((rows_local * sha...  5.99 us

commit v1 on v0

--- a/solution.py
+++ b/solution.py
@@ -174,7 +174,7 @@
     start_hop(0, 1)
 
     steps = [(m, k) for m in range(2) for k in range(4)]
-    diag_by_x = {(0, 0), (1, 0), (0, 2), (1, 2)}
+    diag_by_x = {(0, 2), (1, 2)}
 
     def copies(m, k):
         r = xor2(z, k)

time: 129 us -> 135 us (1.047)
  Pallas kernels: 126 us -> 131 us
    pallas_call x1, Pallas kernels: 120 us -> 125 us  [local_kernel(): pl.pallas_call(kernel, out_shape=(pltpu.VMEM((2, rows_local * shards, wid...]
where the time goes in v1:
time: 135 us; the launch traced here: 134 us
  Pallas kernels  131 us (97%)
  local copies, waits for them, and re-layouts  1.53 us (1%)
    pallas_call x1, Pallas kernels, local_kernel(): pl.pallas_call(kernel, out_shape=(pltpu.VMEM((2, rows_local * shards, wid...  125 us
    pallas_call x1, Pallas kernels, local_kernel(): pl.pallas_call(deliver, out_shape=(jax.ShapeDtypeStruct((rows_local * sha...  5.99 us

profile of v1, /device:TPU:3, one launch (start us, length us, event | category | flops | bytes accessed | tf_op | source)
XLA Modules:
  0.0 133.7 jit_solution(1781974333844070567)
XLA Ops:
  0.6 1.5 %copy.7.gain_hbm = f32[512,1]{1,0:T(8,128)} copy(f32[512,1]{0,1:T(1,128)} %bitcast.1) | data formatting | bytes 4096 | tf_op jit(solution)/shard_map/broadcast_in_dim | solution.py:388
  2.2 125.5 %shard_map.67 = (bf16[2,2048,2048]{2,1,0:T(8,128)(2,1)S(1)}, bf16[192,512]{1,0:T(8,128)(2,1)S(1)}) custom-call(bf16[192,2048]{1,0:T(8,128)(2,1)} %tokens_hbm.1, f32[512,1]{1,0:T(8,128)} %copy.7.gain_hbm, f32[512,2048]{1,0:T(8,128)} %up_hbm.1, f32[512,2048]{1,0:T(8,128)} %down_hbm.1), custom_call_target="tpu_custom_call" | custom-call | tf_op jit(solution)/shard_map/pallas_call | solution.py:359
  127.7 6.0 %shard_map.68 = (bf16[2048,2048]{1,0:T(8,128)(2,1)}, bf16[2048,2048]{1,0:T(8,128)(2,1)}, bf16[192,512]{1,0:T(8,128)(2,1)}) custom-call(bf16[2,2048,2048]{2,1,0:T(8,128)(2,1)S(1)} %get-tuple-element.5.whole, bf16[192,512]{1,0:T(8,128)(2,1)S(1)} %get-tuple-element.6.prompt), custom_call_target="tpu_custom_call" | custom-call | tf_op jit(solution)/shard_map/pallas_call | solution.py:390

commit v2 on v1

v2 whole, which is shorter than its diff:
```python
import jax
import jax.numpy as jnp
from jax import lax
from jax.experimental import pallas as pl
from jax.experimental.pallas import tpu as pltpu
from jax.sharding import PartitionSpec as P

epsilon = 1e-06
MESH = pl.DeviceIdType.MESH

GET, GET_RELAY, SWAP, HOP, HOP_RELAY, SEND_X, SEND_Y, SEND_CORE = range(8)
CAST_ORDER = ((0, 0), (0, 1), (1, 0), (1, 1))
CAST_BOTH = True
ORDER = (((0, 0, 0, 0, 1, 1, 1, 1), (3, 3, 3, 3, 2, 2, 3, 3), (2, 2, 1, 1, 3, 3, 2, 2), (1, 1, 2, 2, 0, 0, 0, 0)), ((1, 1, 3, 3, 3, 3, 2, 2), (3, 3, 1, 1, 2, 2, 3, 3), (2, 2, 2, 2, 0, 0, 0, 0), (0, 0, 0, 0, 1, 1, 1, 1)))
SCHEDULE = (
    (
        ((7,0,0,0,0),),
        ((5,0,0,1,0),),
        (),
        ((7,0,0,1,0),),
        (),
        (),
        ((7,0,0,0,1),),
        (),
        (),
        ((7,0,0,1,1),),
        (),
        (),
        ((7,0,0,2,0),),
        (),
        (),
        ((7,0,0,2,1),),
        ((7,0,0,3,0),(5,0,0,0,1),(7,0,0,3,1),(7,1,0,0,0),(7,1,0,0,1),(7,1,0,1,0),(7,1,0,1,1),),
        ((7,1,0,2,0),(7,1,0,2,1),(7,1,0,3,0),(7,1,0,3,1),(0,0,1,0,0),(7,0,1,0,0),(1,0,0,0,0),(4,0,0,0,0),
        (5,0,0,3,1),(5,0,0,2,0),(0,0,2,0,0),(6,0,2,0,0),(7,0,2,0,0),(0,0,3,1,0),(6,0,3,1,0),(7,0,3,1,0),
        (0,0,1,1,0),(7,0,1,1,0),(5,0,0,2,1),(1,0,0,0,1),(4,0,0,0,1),(0,0,2,0,1),(7,0,2,0,1),(0,0,1,2,0),
        (7,0,1,2,0),(0,0,3,1,1),(7,0,3,1,1),(5,0,3,1,1),(5,0,1,0,0),(0,0,2,1,0),(6,0,2,1,0),(7,0,2,1,0),
        (0,0,3,2,0),(5,0,3,2,0),(7,0,3,2,0),(0,0,1,3,0),(7,0,1,3,0),(5,0,1,1,0),(1,1,0,0,1),(4,1,0,0,1),
        (0,0,3,0,0),(7,0,3,0,0),(0,0,2,1,1),(7,0,2,1,1),(5,0,2,0,0),(0,1,1,0,0),(7,1,1,0,0),(0,0,2,2,0),
        (7,0,2,2,0),(5,0,2,1,0),(0,1,2,0,0),(6,1,2,0,0),(7,1,2,0,0),(5,0,1,2,0),(0,1,1,1,0),(7,1,1,1,0),
        (0,0,1,0,1),(7,0,1,0,1),(5,0,1,3,0),(1,1,0,0,0),(4,1,0,0,0),(0,1,2,0,1),(7,1,2,0,1),(0,0,3,3,0),
        (6,0,3,3,0),(7,0,3,3,0),(0,0,1,2,1),(7,0,1,2,1),(5,1,1,0,0),(0,0,3,0,1),(7,0,3,0,1),(0,0,3,2,1),
        (7,0,3,2,1),(5,1,1,1,0),(0,0,3,3,1),(7,0,3,3,1),),
        ((0,0,2,3,1),(6,0,2,3,1),(7,0,2,3,1),(0,1,2,1,0),(7,1,2,1,0),(6,1,2,1,0),(5,1,2,0,0),(0,0,1,3,1),
        (7,0,1,3,1),(0,0,2,2,1),(7,0,2,2,1),(5,1,2,1,0),(0,0,2,3,0),(7,0,2,3,0),),
        ((0,1,1,2,0),(7,1,1,2,0),(0,1,3,1,0),(6,1,3,1,0),(7,1,3,1,0),(0,0,1,1,1),(7,0,1,1,1),),
        ((5,1,1,2,0),(0,1,2,1,1),(7,1,2,1,1),(0,1,3,3,0),(6,1,3,3,0),(7,1,3,3,0),(0,1,1,3,0),(7,1,1,3,0),
        (0,1,3,1,1),(7,1,3,1,1),(5,1,3,1,1),(0,1,3,3,1),(7,1,3,3,1),(0,1,1,2,1),(7,1,1,2,1),(0,1,3,2,0),
        (5,1,3,2,0),(7,1,3,2,0),(0,1,1,0,1),(7,1,1,0,1),(5,1,1,3,0),(0,1,1,3,1),(7,1,1,3,1),(0,1,1,1,1),
        (7,1,1,1,1),),
        ((5,1,0,0,1),(0,1,3,0,0),(7,1,3,0,0),(5,1,0,1,0),(5,1,0,3,1),(0,1,3,0,1),(7,1,3,0,1),(5,1,0,2,0),
        (0,1,2,2,0),(7,1,2,2,0),(5,1,0,2,1),(0,1,3,2,1),(7,1,3,2,1),),
        ((0,1,2,3,1),(6,1,2,3,1),(7,1,2,3,1),(0,1,2,2,1),(7,1,2,2,1),(0,1,2,3,0),(7,1,2,3,0),),
        (),
        (),
    ),
    (
        ((3,0,0,0,0),),
        ((2,0,0,1,0),),
        ((3,0,0,2,0),),
        (),
        (),
        (),
        (),
        (),
        (),
        (),
        (),
        (),
        (),
        (),
        (),
        (),
        ((3,0,0,3,0),(2,1,0,1,0),),
        ((1,0,0,0,0),(4,0,0,0,0),(1,0,0,3,0),(4,0,0,3,0),(1,1,0,3,0),(4,1,0,3,0),(3,1,0,0,0),),
        ((1,1,0,0,0),(4,1,0,0,0),),
        (),
        ((3,1,0,2,0),(3,0,0,3,1),(3,1,0,3,0),(3,1,0,3,1),),
        (),
        (),
        (),
        (),
    ),
    (
        ((2,0,0,0,0),),
        ((3,0,0,1,0),),
        (),
        (),
        (),
        (),
        (),
        (),
        (),
        (),
        (),
        (),
        (),
        (),
        (),
        (),
        ((2,0,0,0,1),(0,0,0,1,0),(6,0,0,1,0),(7,0,0,1,0),(2,1,0,0,1),(3,0,0,2,0),(0,0,0,1,1),(7,0,0,1,1),
        (0,0,0,0,1),(6,0,0,0,1),(7,0,0,0,1),(2,1,0,0,0),(0,0,0,3,1),(6,0,0,3,1),(7,0,0,3,1),(0,0,0,0,0),
        (7,0,0,0,0),(0,0,0,2,0),(7,0,0,2,0),(0,0,2,2,0),(7,0,2,2,0),(0,0,0,3,0),(7,0,0,3,0),(3,0,0,3,0),
        (0,0,0,2,1),(7,0,0,2,1),),
        ((0,0,3,0,0),(6,0,3,0,0),(7,0,3,0,0),(5,0,3,0,0),(5,0,2,2,0),(0,0,3,1,1),(7,0,3,1,1),(6,0,3,1,1),
        (0,0,3,0,1),(7,0,3,0,1),(0,0,1,0,0),(7,0,1,0,0),(6,0,1,0,0),(0,0,3,1,0),(7,0,3,1,0),(3,1,0,1,0),
        (0,0,3,2,0),(7,0,3,2,0),(6,0,3,2,0),(0,0,2,3,0),(7,0,2,3,0),(6,0,2,3,0),(0,0,1,0,1),(5,0,1,0,1),
        (7,0,1,0,1),(0,0,1,1,0),(7,0,1,1,0),(0,0,3,3,0),(7,0,3,3,0),(5,0,3,3,0),(6,0,3,3,0),(0,0,3,2,1),
        (7,0,3,2,1),(5,0,3,2,1),(0,0,2,0,0),(7,0,2,0,0),(6,0,1,1,0),(0,0,2,3,1),(7,0,2,3,1),(5,0,2,3,1),
        (0,0,2,1,0),(7,0,2,1,0),(0,0,3,3,1),(7,0,3,3,1),),
        ((3,1,0,2,0),(0,0,1,2,0),(7,0,1,2,0),(6,0,1,2,0),(0,0,2,2,1),(7,0,2,2,1),(5,0,2,2,1),(0,0,1,1,1),
        (7,0,1,1,1),(5,0,1,1,1),(0,0,1,3,0),(7,0,1,3,0),(6,0,1,3,0),(0,1,3,3,0),(7,1,3,3,0),(6,1,3,3,0),
        (5,1,3,3,0),(0,0,1,2,1),(7,0,1,2,1),(0,1,1,0,0),(7,1,1,0,0),(6,1,1,0,0),(0,0,1,3,1),(7,0,1,3,1),),
        ((3,0,0,3,1),(0,1,1,1,0),(7,1,1,1,0),(6,1,1,1,0),(0,1,3,3,1),(7,1,3,3,1),(0,0,2,0,1),(7,0,2,0,1),
        (0,1,2,0,0),(7,1,2,0,0),(0,1,1,0,1),(5,1,1,0,1),(7,1,1,0,1),(0,1,2,1,0),(7,1,2,1,0),(3,1,0,3,0),
        (0,1,1,1,1),(5,1,1,1,1),(7,1,1,1,1),(0,1,3,0,0),(6,1,3,0,0),(7,1,3,0,0),(5,1,3,0,0),(0,1,1,2,0),
        (6,1,1,2,0),(7,1,1,2,0),(0,0,2,1,1),(7,0,2,1,1),),
        ((0,1,3,1,1),(7,1,3,1,1),(6,1,3,1,1),(0,1,3,0,1),(7,1,3,0,1),(3,1,0,3,1),(0,1,3,2,0),(7,1,3,2,0),
        (6,1,3,2,0),(0,1,1,2,1),(7,1,1,2,1),(0,1,2,3,0),(7,1,2,3,0),(6,1,2,3,0),(0,1,1,3,0),(7,1,1,3,0),
        (0,1,3,1,0),(7,1,3,1,0),(0,1,2,2,0),(5,1,2,2,0),(7,1,2,2,0),(6,1,1,3,0),(0,1,0,0,1),(7,1,0,0,1),
        (0,1,3,2,1),(7,1,3,2,1),(5,1,3,2,1),),
        ((0,1,2,2,1),(7,1,2,2,1),(6,1,0,0,1),(0,1,0,1,0),(7,1,0,1,0),(5,1,2,2,1),(0,1,2,3,1),(7,1,2,3,1),
        (5,1,2,3,1),(0,1,2,0,1),(7,1,2,0,1),(6,1,0,1,0),(0,1,0,3,1),(7,1,0,3,1),(0,1,1,3,1),(7,1,1,3,1),),
        ((0,1,2,1,1),(7,1,2,1,1),(6,1,0,3,1),),
        ((0,1,0,2,0),(7,1,0,2,0),(0,1,0,0,0),(7,1,0,0,0),(0,1,0,2,1),(7,1,0,2,1),(0,1,0,1,1),(7,1,0,1,1),
        (0,1,0,3,0),(7,1,0,3,0),),
        (),
    ),
    (
        ((2,0,0,0,0),),
        ((3,0,0,1,0),),
        (),
        (),
        (),
        (),
        (),
        (),
        (),
        (),
        (),
        (),
        (),
        (),
        (),
        (),
        ((2,0,0,3,0),(2,1,0,3,0),(3,0,0,2,0),(2,1,0,0,0),(1,0,0,1,0),(4,0,0,1,0),),
        ((3,0,0,0,1),(3,1,0,1,0),),
        ((3,1,0,2,0),),
        ((1,1,0,1,0),(4,1,0,1,0),(3,1,0,0,1),),
        (),
        (),
        (),
        (),
        (),
    ),
    (
        ((3,0,1,0,0),),
        (),
        (),
        (),
        (),
        (),
        (),
        (),
        (),
        (),
        (),
        (),
        (),
        (),
        (),
        (),
        ((3,0,1,1,0),),
        ((1,0,1,2,0),(4,0,1,2,0),(3,0,1,2,0),(3,0,1,3,0),(1,0,1,1,1),(4,0,1,1,1),(3,1,1,0,0),(3,1,1,1,0),
        (1,0,1,3,0),(4,0,1,3,0),(3,0,1,2,1),(3,0,1,3,1),(1,1,1,2,0),(4,1,1,2,0),(3,1,1,2,0),(3,1,1,3,0),
        (1,1,1,1,1),(4,1,1,1,1),(3,1,1,2,1),),
        ((3,1,1,3,1),(1,1,1,3,0),(4,1,1,3,0),),
        (),
        (),
        (),
        (),
        (),
        (),
    ),
    (
        ((7,0,1,0,0),),
        ((5,0,1,1,0),),
        (),
        ((7,0,1,1,0),),
        ((5,0,1,0,1),),
        (),
        ((7,0,1,0,1),),
        (),
        (),
        ((7,0,1,1,1),),
        (),
        (),
        ((7,0,1,2,0),),
        (),
        (),
        ((7,0,1,2,1),),
        ((7,0,1,3,0),(5,0,1,2,1),(7,0,1,3,1),(7,1,1,0,0),(7,1,1,0,1),(0,0,0,0,0),(7,0,0,0,0),(7,1,1,1,0),),
        ((7,1,1,1,1),(7,1,1,2,0),(5,0,1,3,1),(7,1,1,2,1),(7,1,1,3,0),(7,1,1,3,1),(0,0,0,2,0),(6,0,0,2,0),
        (7,0,0,2,0),(1,0,1,2,0),(4,0,1,2,0),(5,0,0,0,0),(0,0,0,3,0),(7,0,0,3,0),(0,0,0,2,1),(7,0,0,2,1),
        (0,0,2,0,0),(6,0,2,0,0),(7,0,2,0,0),(5,0,2,0,0),(0,0,3,1,0),(6,0,3,1,0),(7,0,3,1,0),(1,0,1,3,0),
        (4,0,1,3,0),(0,0,2,0,1),(7,0,2,0,1),(5,0,2,0,1),(0,0,3,1,1),(7,0,3,1,1),(5,0,3,1,1),(5,0,0,2,1),
        (5,0,0,3,0),(0,0,2,3,1),(6,0,2,3,1),(7,0,2,3,1),(0,0,3,2,0),(6,0,3,2,0),(7,0,3,2,0),(5,1,1,0,1),
        (1,0,1,2,1),(4,0,1,2,1),(0,0,2,3,0),(7,0,2,3,0),(0,0,3,2,1),(7,0,3,2,1),(5,0,3,2,1),(0,0,2,1,0),
        (7,0,2,1,0),(5,1,1,1,0),(0,0,3,3,0),(5,0,3,3,0),(7,0,3,3,0),(5,1,1,2,1),(1,0,1,0,1),(4,0,1,0,1),
        (0,0,3,0,1),(6,0,3,0,1),(7,0,3,0,1),(5,1,1,3,1),(0,0,0,1,0),(6,0,0,1,0),(7,0,0,1,0),(0,0,3,0,0),
        (7,0,3,0,0),(0,0,2,2,1),(6,0,2,2,1),(7,0,2,2,1),(0,1,2,0,0),(7,1,2,0,0),(0,1,3,1,0),(6,1,3,1,0),
        (5,1,2,0,0),(0,0,0,1,1),(5,0,0,1,1),(7,0,0,1,1),(7,1,3,1,0),(6,1,2,0,0),(0,0,2,1,1),(7,0,2,1,1),
        (1,0,1,1,1),(4,0,1,1,1),(0,0,2,2,0),(7,0,2,2,0),),
        ((0,1,0,0,0),(7,1,0,0,0),(5,1,0,0,0),(0,1,3,1,1),(7,1,3,1,1),(5,1,3,1,1),(0,1,2,3,1),(6,1,2,3,1),
        (7,1,2,3,1),(0,1,3,2,0),(6,1,3,2,0),(0,1,2,0,1),(5,1,2,0,1),(7,1,3,2,0),(7,1,2,0,1),(1,1,1,3,0),
        (4,1,1,3,0),(0,1,2,3,0),(7,1,2,3,0),(0,0,0,0,1),(7,0,0,0,1),(0,1,3,2,1),(5,1,3,2,1),(7,1,3,2,1),
        (1,1,1,2,0),(4,1,1,2,0),(0,1,0,2,0),(6,1,0,2,0),(0,0,3,3,1),(7,0,3,3,1),),
        ((0,1,3,0,1),(6,1,3,0,1),(7,1,3,0,1),(0,1,2,1,0),(7,1,2,1,0),(7,1,0,2,0),(1,1,1,2,1),(4,1,1,2,1),
        (0,0,0,3,1),(7,0,0,3,1),),
        ((0,1,0,2,1),(5,1,0,2,1),(7,1,0,2,1),(1,1,1,0,1),(4,1,1,0,1),(0,1,0,3,0),(7,1,0,3,0),(0,1,3,3,0),
        (5,1,3,3,0),(0,1,2,2,1),(6,1,2,2,1),(7,1,3,3,0),(7,1,2,2,1),(5,1,0,3,0),(0,1,3,0,0),(7,1,3,0,0),
        (1,1,1,1,1),(4,1,1,1,1),(0,1,0,3,1),(7,1,0,3,1),(0,1,0,1,0),(6,1,0,1,0),(7,1,0,1,0),(0,1,3,3,1),
        (7,1,3,3,1),),
        ((0,1,2,2,0),(7,1,2,2,0),(0,1,2,1,1),(7,1,2,1,1),),
        ((0,1,0,1,1),(5,1,0,1,1),(7,1,0,1,1),(0,1,0,0,1),(7,1,0,0,1),),
        (),
        (),
    ),
    (
        ((3,0,1,0,0),),
        (),
        ((2,0,1,2,0),),
        (),
        (),
        (),
        (),
        (),
        (),
        (),
        (),
        (),
        (),
        (),
        (),
        (),
        ((2,0,1,1,1),(3,0,1,3,1),(2,0,1,3,0),(2,1,1,2,0),),
        ((3,0,1,1,0),(2,1,1,1,1),(2,1,1,3,0),(3,1,1,0,0),(3,1,1,3,1),),
        ((3,1,1,1,0),),
        (),
        (),
        (),
        (),
        (),
        (),
    ),
    (
        ((3,0,1,0,0),),
        (),
        ((2,0,1,2,0),),
        (),
        (),
        (),
        (),
        (),
        (),
        (),
        (),
        (),
        (),
        (),
        (),
        (),
        ((2,0,1,3,0),(0,0,1,1,0),(6,0,1,1,0),(7,0,1,1,0),(0,0,1,0,1),(6,0,1,0,1),(7,0,1,0,1),(3,0,1,1,0),
        (0,0,1,1,1),(7,0,1,1,1),(2,0,1,2,1),(0,0,1,2,1),(6,0,1,2,1),(7,0,1,2,1),(0,0,1,0,0),(7,0,1,0,0),
        (0,0,1,3,1),(6,0,1,3,1),(7,0,1,3,1),(0,0,1,2,0),(7,0,1,2,0),(2,0,1,0,1),(0,0,0,0,0),(6,0,0,0,0),
        (7,0,0,0,0),(0,0,1,3,0),(7,0,1,3,0),),
        ((0,0,2,0,0),(7,0,2,0,0),(0,0,3,0,0),(7,0,3,0,0),(0,0,2,2,0),(6,0,2,2,0),(7,0,2,2,0),(3,1,1,0,0),
        (0,0,0,0,1),(7,0,0,0,1),(2,0,1,1,1),(0,0,2,0,1),(7,0,2,0,1),(0,0,2,2,1),(7,0,2,2,1),(0,0,3,1,1),
        (6,0,3,1,1),(7,0,3,1,1),(2,1,1,3,0),(0,0,0,2,1),(6,0,0,2,1),(7,0,0,2,1),(0,0,3,1,0),(7,0,3,1,0),
        (0,0,0,1,0),(7,0,0,1,0),(3,1,1,1,0),(0,0,0,3,0),(6,0,0,3,0),(7,0,0,3,0),(0,0,3,0,1),(7,0,3,0,1),
        (0,0,2,1,1),(6,0,2,1,1),(7,0,2,1,1),(0,0,0,2,0),(7,0,0,2,0),(5,0,3,0,1),(0,1,1,0,1),(7,1,1,0,1),
        (0,0,0,3,1),(7,0,0,3,1),(5,0,0,1,0),(0,0,3,2,1),(6,0,3,2,1),(7,0,3,2,1),(0,0,2,1,0),(7,0,2,1,0),
        (5,0,2,2,1),(6,1,1,0,1),(0,0,3,3,0),(6,0,3,3,0),(7,0,3,3,0),(0,0,3,2,0),(7,0,3,2,0),(5,0,2,1,1),
        (0,1,1,1,0),(7,1,1,1,0),(0,1,3,0,1),(7,1,3,0,1),(0,0,2,3,0),(6,0,2,3,0),(7,0,2,3,0),(0,0,3,3,1),
        (7,0,3,3,1),),
        ((2,1,1,2,0),(6,1,1,1,0),(0,1,1,2,1),(7,1,1,2,1),(0,1,1,0,0),(7,1,1,0,0),(2,1,1,2,1),(6,1,1,2,1),
        (0,1,1,3,1),(7,1,1,3,1),(0,0,2,3,1),(7,0,2,3,1),),
        ((2,1,1,0,1),(0,0,0,1,1),(7,0,0,1,1),),
        ((0,1,1,1,1),(7,1,1,1,1),(5,0,0,0,1),(0,1,3,0,0),(7,1,3,0,0),(0,1,2,2,0),(6,1,2,2,0),(7,1,2,2,0),
        (0,1,2,0,0),(7,1,2,0,0),(0,1,1,2,0),(7,1,1,2,0),(5,1,3,0,1),(0,1,3,1,1),(6,1,3,1,1),(7,1,3,1,1),
        (0,1,2,2,1),(7,1,2,2,1),(2,1,1,1,1),(0,1,0,0,0),(6,1,0,0,0),(7,1,0,0,0),(0,1,3,1,0),(7,1,3,1,0),
        (0,1,2,1,1),(6,1,2,1,1),(5,1,2,2,1),(7,1,2,1,1),(6,1,1,3,1),(0,1,2,0,1),(7,1,2,0,1),(0,1,0,0,1),
        (7,1,0,0,1),(0,1,0,1,0),(7,1,0,1,0),(5,1,0,1,0),(0,1,3,2,1),(7,1,3,2,1),(6,1,3,2,1),(0,1,2,1,0),
        (7,1,2,1,0),(5,1,2,1,1),(0,1,2,3,0),(7,1,2,3,0),(6,1,2,3,0),(0,1,1,3,0),(7,1,1,3,0),(5,1,0,0,1),
        (0,1,0,2,1),(7,1,0,2,1),(0,1,3,2,0),(7,1,3,2,0),(0,1,3,3,0),(7,1,3,3,0),(6,1,3,3,0),(6,1,0,2,1),
        (0,1,2,3,1),(7,1,2,3,1),),
        ((0,1,0,3,0),(7,1,0,3,0),(6,1,0,3,0),(0,1,3,3,1),(7,1,3,3,1),),
        ((0,1,0,1,1),(7,1,0,1,1),(0,1,0,2,0),(7,1,0,2,0),(0,1,0,3,1),(7,1,0,3,1),),
        (),
        (),
    ),
)


def local_plain(tokens, norm_gain, up_trained, down_trained):
    shards = lax.axis_size("fs")
    groups = lax.axis_size("tp")
    rows_local = up_trained.shape[0]
    cols_local = up_trained.shape[1]
    folded = (norm_gain[:, None] * up_trained).astype(jnp.bfloat16)
    stacked = jnp.stack([folded, down_trained.astype(jnp.bfloat16)])
    served_width = cols_local * groups // shards
    blocks_here = cols_local // served_width
    quarter_rows = rows_local // groups
    pieces = stacked.reshape(2, groups, quarter_rows, blocks_here, served_width)
    moved = lax.all_to_all(pieces, "tp", split_axis=1, concat_axis=3, tiled=True)
    placed = lax.all_to_all(moved, "fs", split_axis=3, concat_axis=2, tiled=True)
    ordered = placed.reshape(2, shards, quarter_rows, served_width)
    joined = lax.all_gather(ordered, "tp", axis=2, tiled=True)
    owned = joined.reshape(2, rows_local * shards, served_width)
    up_serving = owned[0]
    down_serving = owned[1]
    values = tokens.astype(jnp.float32)
    scale = lax.rsqrt(jnp.mean(values * values, axis=1, keepdims=True) + epsilon)
    normed = (values * scale).astype(jnp.bfloat16)
    hidden = jnp.dot(normed, up_serving, preferred_element_type=jnp.float32)
    active = jnp.square(jax.nn.relu(hidden)).astype(jnp.bfloat16)
    summed = lax.psum_scatter(
        lax.dot_general(
            down_serving, active, (((1,), (1,)), ((), ())), preferred_element_type=jnp.float32
        ),
        "fs",
        scatter_dimension=0,
        tiled=True,
    )
    prompt_output = summed.T.astype(jnp.bfloat16)
    return (up_serving, down_serving, prompt_output)


def kernel(
    tokens_hbm, gain_hbm, up_hbm, down_hbm, whole, prompt_out,
    raw, gain_rows, gain, cast, relay, toks, normed, hidden, active, rs_send, rs_recv, rs_own,
    in_sem, misc_sem, got_sem, relay_sem, block_sem, src_sem, out_sem, rs_ssem, rs_rsem,
):
    y = lax.axis_index("grp")
    z = lax.axis_index("fs")
    t = lax.axis_index("tp")
    mirrored = z // 2
    role = jnp.where(mirrored == 1, 4 * (3 - z) + (3 - t), 4 * z + t)
    is_own = z == t
    is_active = t % 2 == z % 2
    t_x = jnp.where(t < 2, t + 2, t - 2)
    t_c = t + 1 - 2 * (t % 2)
    to_x = {"tp": t_x}
    to_c = {"tp": t_c}
    to_y = {"grp": 1 - y}
    rows_local, width = cast.shape[1], cast.shape[2]
    size = rows_local // 8
    trained = (up_hbm, down_hbm)
    planes = [jnp.where(mirrored == 1, 3 - k, k) for k in range(4)]
    sides = [y, 1 - y]

    def part(pair, side):
        return 2 * pair + sides[side]

    def ds(start, extent):
        return pl.ds(pl.multiple_of(start, extent), extent)

    def local_rows(pair, side):
        return ds(part(pair, side) * size, size)

    def unit(m, plane, pair, side):
        return whole.at[m, ds(plane * rows_local + part(pair, side) * size, size)]

    def remote(src, dst, ssem, rsem, where):
        return pltpu.make_async_remote_copy(
            src_ref=src, dst_ref=dst, send_sem=ssem, recv_sem=rsem,
            device_id=where, device_id_type=MESH,
        )

    def fetch(m, pair, side):
        rows = local_rows(pair, side)
        return pltpu.make_async_copy(
            trained[m].at[rows], raw.at[m, rows], in_sem.at[m, 2 * pair + side]
        )

    get_gain = pltpu.make_async_copy(gain_hbm, gain_rows, misc_sem.at[0])
    get_toks = pltpu.make_async_copy(tokens_hbm, toks, misc_sem.at[1])
    get_gain.start()
    for m, side in CAST_ORDER:
        def start_fetches():
            for pair in range(4):
                fetch(m, pair, side).start()
        if side == 0 or CAST_BOTH:
            start_fetches()
        else:
            pl.when(is_own)(start_fetches)
    get_toks.start()

    barrier = pltpu.get_barrier_semaphore()
    others = [{"fs": lax.rem(z + k, 4)} for k in range(1, 4)]
    for where in [to_x, to_c, to_y] + others:
        pl.semaphore_signal(barrier, inc=1, device_id=where, device_id_type=MESH)

    get_gain.wait()
    lanes = gain_rows.shape[1]
    for q in range(gain_rows.shape[0]):
        square = (lanes, lanes)
        chosen = jnp.where(
            lax.broadcasted_iota(jnp.int32, square, 0) == lax.broadcasted_iota(jnp.int32, square, 1),
            jnp.broadcast_to(gain_rows[pl.ds(q, 1), :], square), 0.0,
        )
        gain[pl.ds(q * lanes, lanes), :] = jnp.sum(chosen, axis=1, keepdims=True)

    piece = 16

    def cast_unit(m, pair, side):
        fetch(m, pair, side).wait()
        base = part(pair, side) * size

        def store(into, shift):
            @pl.loop(0, size // piece)
            def _(i):
                here = ds(base + i * piece, piece)
                values = raw[m, here, :]
                if m == 0:
                    values = values * gain[here, :]
                into[m, ds(shift + base + i * piece, piece), :] = values.astype(jnp.bfloat16)

        @pl.when(is_own)
        def _():
            store(whole, z * rows_local)

        if side == 0 or CAST_BOTH:
            @pl.when(jnp.logical_not(is_own))
            def _():
                store(cast, 0)

    def step(kind, m, k, pair, side):
        plane = planes[k]
        place = part(pair, side)
        if kind == GET:
            here = unit(m, plane, pair, side)
            remote(here, here, out_sem.at[0, m], got_sem.at[m, plane, place], to_x).wait_recv()
        elif kind == GET_RELAY:
            here = relay.at[m, ds(place * size, size)]
            remote(here, here, src_sem.at[m], relay_sem.at[m, place], to_x).wait_recv()
        elif kind == SWAP:
            remote(
                cast.at[m, local_rows(pair, side)], relay.at[m, ds(place * size, size)],
                src_sem.at[m], relay_sem.at[m, place], to_x,
            ).start()
        elif kind in (HOP, HOP_RELAY):
            src = (cast if kind == HOP else relay).at[m, ds(place * size, size)]
            remote(
                src, unit(m, z, pair, side), src_sem.at[m], got_sem.at[m, z, place],
                {"fs": t if kind == HOP else t_x},
            ).start()
        elif kind == SEND_CORE:
            here = unit(m, plane, pair, side)
            remote(here, here, out_sem.at[2, m], block_sem.at[m, plane], to_c).start()
        else:
            here = unit(m, plane, pair, side)
            i = kind - SEND_X
            remote(
                here, here, out_sem.at[i, m], got_sem.at[m, plane, place], (to_x, to_y)[i]
            ).start()

    def run(segment):
        for r in range(8):
            if SCHEDULE[r][segment]:
                @pl.when(role == r)
                def _():
                    for s in SCHEDULE[r][segment]:
                        step(*s)

    casts = [(m, pair, side) for m, side in CAST_ORDER for pair in range(4)]
    first = True
    segment = 0
    for m, pair, side in casts:
        if side == 1 and not CAST_BOTH:
            pl.when(is_own)(lambda: cast_unit(m, pair, side))
        else:
            cast_unit(m, pair, side)
        if first:
            pl.semaphore_wait(barrier, 6)
            first = False
        run(segment)
        segment += 1

    get_toks.wait()
    tokens_here = toks.shape[0]

    @pl.loop(0, tokens_here // piece)
    def _(i):
        here = ds(i * piece, piece)
        values = toks[here, :].astype(jnp.float32)
        scale = lax.rsqrt(jnp.mean(values * values, axis=1, keepdims=True) + epsilon)
        normed[here, :] = (values * scale).astype(jnp.bfloat16)

    def pick(table):
        chosen = planes[table[0]]
        for r in range(1, 8):
            if table[r] != table[0]:
                chosen = jnp.where(role == r, planes[table[r]], chosen)
        return chosen

    def listen(m, plane):
        @pl.when(jnp.logical_not(is_active))
        def _():
            here = whole.at[m, ds(plane * rows_local, rows_local)]
            remote(here, here, out_sem.at[2, m], block_sem.at[m, plane], to_c).wait_recv()

    tile = 512 if width % 512 == 0 else width

    def compute_up(k):
        plane = pick(ORDER[0][k])
        listen(0, plane)
        rows = ds(plane * rows_local, rows_local)

        @pl.loop(0, width // tile)
        def _(n):
            cols = ds(n * tile, tile)
            product = jnp.dot(
                normed[:, rows], whole[0, rows, cols], preferred_element_type=jnp.float32
            )
            if k > 0:
                product = product + hidden[:, cols]
            if k < 3:
                hidden[:, cols] = product
            else:
                active[:, cols] = jnp.square(jnp.maximum(product, 0.0)).astype(jnp.bfloat16)

    d_tile = 256 if rows_local % 256 == 0 else rows_local

    def scatter(k, plane):
        slot = lax.rem(z - plane + 3, 4)
        return remote(
            rs_send.at[k], rs_recv.at[slot], rs_ssem.at[k], rs_rsem.at[slot], {"fs": plane}
        )

    def compute_down(k):
        plane = pick(ORDER[1][k])
        listen(1, plane)

        @pl.loop(0, rows_local // d_tile)
        def _(n):
            cols = ds(n * d_tile, d_tile)
            product = lax.dot_general(
                active[...], whole[1, ds(plane * rows_local + n * d_tile, d_tile), :],
                (((1,), (1,)), ((), ())), preferred_element_type=jnp.float32,
            )
            if k < 3:
                rs_send[k, :, cols] = product.astype(jnp.bfloat16)
            else:
                rs_own[:, cols] = product
        if k < 3:
            scatter(k, plane).start()

    for m in range(2):
        for k in range(4):
            run(segment)
            segment += 1
            (compute_up, compute_down)[m](k)
    run(segment)

    for k in range(3):
        here = rs_recv.at[k]
        remote(here, here, rs_ssem.at[k], rs_rsem.at[k], {"fs": lax.rem(z + 1, 4)}).wait_recv()

    @pl.loop(0, tokens_here // piece)
    def _(i):
        here = ds(i * piece, piece)
        total = rs_own[here, :]
        for k in range(3):
            total = total + rs_recv[k, here, :].astype(jnp.float32)
        prompt_out[here, :] = total.astype(prompt_out.dtype)

    def drain(sem, m, count):
        sent = whole.at[m, pl.ds(0, count * size)]
        remote(sent, sent, sem, got_sem.at[0, 0, 0], to_x).wait_send()

    for r in range(8):
        @pl.when(role == r)
        def _():
            for m in range(2):
                steps = [s for part_of in SCHEDULE[r] for s in part_of if s[1] == m]
                hops = sum(s[0] in (SWAP, HOP, HOP_RELAY) for s in steps)
                if hops:
                    drain(src_sem.at[m], m, hops)
                for i, kind in enumerate((SEND_X, SEND_Y, SEND_CORE)):
                    sends = sum(s[0] == kind for s in steps)
                    if sends:
                        drain(out_sem.at[i, m], m, sends)
    for k in range(3):
        here = rs_send.at[k]
        remote(here, here, rs_ssem.at[k], rs_rsem.at[k], {"fs": lax.rem(z + 1, 4)}).wait_send()


pieces_out = 8


def deliver(whole, prompt, up_out, down_out, prompt_out, sems, last):
    rows = whole.shape[1] // pieces_out
    copies = [
        pltpu.make_async_copy(
            whole.at[m, pl.ds(i * rows, rows)], out.at[pl.ds(i * rows, rows)], sems.at[m, i]
        )
        for m, out in enumerate((up_out, down_out))
        for i in range(pieces_out)
    ]
    copies.append(pltpu.make_async_copy(prompt, prompt_out, last))
    for copy in copies:
        copy.start()
    for copy in copies:
        copy.wait()


def local_kernel(tokens, norm_gain, up_trained, down_trained):
    shards = lax.axis_size("fs")
    rows_local, width = up_trained.shape
    tokens_here, features = tokens.shape
    any_space = pl.BlockSpec(memory_space=pl.ANY)
    dma = pltpu.SemaphoreType.DMA
    bf16, f32 = jnp.bfloat16, jnp.float32
    whole, prompt = pl.pallas_call(
        kernel,
        out_shape=(
            pltpu.VMEM((2, rows_local * shards, width), bf16),
            pltpu.VMEM((tokens_here, rows_local), bf16),
        ),
        in_specs=[any_space] * 4,
        out_specs=(pl.BlockSpec(memory_space=pltpu.VMEM),) * 2,
        scratch_shapes=[
            pltpu.VMEM((2, rows_local, width), f32),
            pltpu.VMEM((rows_local // 128, 128), f32),
            pltpu.VMEM((rows_local, 1), f32),
            pltpu.VMEM((2, rows_local, width), bf16),
            pltpu.VMEM((2, rows_local, width), bf16),
            pltpu.VMEM((tokens_here, features), bf16),
            pltpu.VMEM((tokens_here, features), bf16),
            pltpu.VMEM((tokens_here, width), f32),
            pltpu.VMEM((tokens_here, width), bf16),
            pltpu.VMEM((3, tokens_here, rows_local), bf16),
            pltpu.VMEM((3, tokens_here, rows_local), bf16),
            pltpu.VMEM((tokens_here, rows_local), f32),
            dma((2, 8)), dma((2,)),
            dma((2, 4, 8)), dma((2, 8)), dma((2, 4)),
            dma((2,)), dma((3, 2)), dma((3,)), dma((3,)),
        ],
        compiler_params=pltpu.CompilerParams(
            collective_id=0, has_side_effects=True, vmem_limit_bytes=40 * 1024 * 1024
        ),
    )(tokens, norm_gain.reshape(rows_local // 128, 128), up_trained, down_trained)
    held = pl.BlockSpec(memory_space=pltpu.VMEM)
    return tuple(pl.pallas_call(
        deliver,
        out_shape=(
            jax.ShapeDtypeStruct((rows_local * shards, width), bf16),
            jax.ShapeDtypeStruct((rows_local * shards, width), bf16),
            jax.ShapeDtypeStruct((tokens_here, rows_local), bf16),
        ),
        in_specs=[held, held],
        out_specs=(any_space,) * 3,
        scratch_shapes=[dma((2, pieces_out)), dma(())],
        compiler_params=pltpu.CompilerParams(vmem_limit_bytes=8 * 1024 * 1024),
    )(whole, prompt))


def solution(mesh):
    in_specs = (P(("grp", "tp"), None), P("fs"), P("fs", "tp"), P("fs", "tp"))
    out_specs = (P("grp", "fs"), P("grp", "fs"), P(("grp", "tp"), "fs"))
    sizes = mesh.shape
    square = sizes["grp"] == 2 and sizes["fs"] == 4 and sizes["tp"] == 4
    local = local_kernel if square else local_plain
    return jax.shard_map(local, mesh=mesh, in_specs=in_specs, out_specs=out_specs, check_vma=False)
```

time: 135 us -> 122 us (0.904)
  the two profiles are of different devices: /device:TPU:3 before, /device:TPU:1 now
where the time goes in v2:
time: 122 us; the launch traced here: 121 us
  Pallas kernels  121 us (99%)
    pallas_call x1, Pallas kernels, local_kernel(): pl.pallas_call(kernel, out_shape=(pltpu.VMEM((2, rows_local * shards, wid...  115 us
    pallas_call x1, Pallas kernels, local_kernel(): pl.pallas_call(deliver, out_shape=(jax.ShapeDtypeStruct((rows_local * sha...  5.99 us

profile of v2, /device:TPU:1, one launch (start us, length us, event | category | flops | bytes accessed | tf_op | source)
XLA Modules:
  0.0 121.4 jit_solution(9307897144863211040)
XLA Ops:
  0.6 114.8 %shard_map.67 = (bf16[2,2048,2048]{2,1,0:T(8,128)(2,1)S(1)}, bf16[192,512]{1,0:T(8,128)(2,1)S(1)}) custom-call(bf16[192,2048]{1,0:T(8,128)(2,1)} %tokens_hbm.1, f32[4,128]{1,0:T(4,128)} %bitcast.1, f32[512,2048]{1,0:T(8,128)} %up_hbm.1, f32[512,2048]{1,0:T(8,128)} %down_hbm.1), custom_call_target="tpu_custom_call" | custom-call | tf_op jit(solution)/shard_map/pallas_call | solution.py:626
  115.4 6.0 %shard_map.68 = (bf16[2048,2048]{1,0:T(8,128)(2,1)}, bf16[2048,2048]{1,0:T(8,128)(2,1)}, bf16[192,512]{1,0:T(8,128)(2,1)}) custom-call(bf16[2,2048,2048]{2,1,0:T(8,128)(2,1)S(1)} %get-tuple-element.5.whole, bf16[192,512]{1,0:T(8,128)(2,1)S(1)} %get-tuple-element.6.prompt), custom_call_target="tpu_custom_call" | custom-call | tf_op jit(solution)/shard_map/pallas_call | solution.py:656

commit v3 on v2

v3 whole, which is shorter than its diff:
```python
import jax
import jax.numpy as jnp
from jax import lax
from jax.experimental import pallas as pl
from jax.experimental.pallas import tpu as pltpu
from jax.sharding import PartitionSpec as P

epsilon = 1e-06
MESH = pl.DeviceIdType.MESH

GET, GET_RELAY, SWAP, HOP, HOP_RELAY, SEND_X, SEND_Y, SEND_CORE = range(8)
PAIRS = 4
ORDER = (
    (
        (0, 0, 1, 1, 1, 1, 1, 1),
        (1, 1, 0, 0, 3, 3, 0, 0),
        (2, 2, 3, 3, 0, 0, 3, 3),
        (3, 3, 2, 2, 2, 2, 2, 2),
    ),
    (
        (3, 3, 3, 3, 0, 0, 0, 0),
        (2, 2, 2, 2, 3, 3, 3, 3),
        (1, 1, 1, 1, 2, 2, 2, 2),
        (0, 0, 0, 0, 1, 1, 1, 1),
    ),
)
SCHEDULE = (
    (
        ((5, 0, 0, 0, 0), (7, 0, 0, 0, 0),),
        (),
        (),
        (),
        (),
        ((7, 0, 0, 0, 1),),
        (),
        (),
        (),
        (),
        ((7, 0, 0, 1, 0),),
        (),
        (),
        (),
        (),
        ((5, 0, 0, 1, 1), (7, 0, 0, 1, 1),),
        ((7, 0, 0, 2, 0), (7, 0, 0, 2, 1), (7, 0, 0, 3, 0), (7, 0, 0, 3, 1), (7, 1, 0, 0, 0),),
        ((7, 1, 0, 0, 1), (7, 1, 0, 1, 0), (7, 1, 0, 1, 1), (7, 1, 0, 2, 0), (7, 1, 0, 2, 1),
         (7, 1, 0, 3, 0), (7, 1, 0, 3, 1), (0, 0, 1, 0, 0), (5, 0, 1, 0, 0), (7, 0, 1, 0, 0),
         (1, 0, 0, 1, 0), (4, 0, 0, 1, 0), (0, 0, 3, 2, 0), (7, 0, 3, 2, 0), (5, 0, 3, 2, 0),
         (0, 0, 1, 1, 0), (7, 0, 1, 1, 0), (5, 0, 1, 1, 0), (1, 0, 0, 2, 0), (4, 0, 0, 2, 0),
         (5, 0, 0, 2, 1), (0, 1, 3, 1, 0), (6, 1, 3, 1, 0), (7, 1, 3, 1, 0), (0, 0, 1, 2, 0),
         (7, 0, 1, 2, 0), (5, 0, 1, 2, 0), (1, 0, 0, 3, 0), (4, 0, 0, 3, 0), (0, 1, 3, 1, 1),
         (7, 1, 3, 1, 1), (5, 0, 0, 3, 1), (0, 1, 3, 3, 0), (7, 1, 3, 3, 0), (5, 1, 3, 3, 0),
         (0, 0, 1, 3, 0), (7, 0, 1, 3, 0), (1, 1, 0, 1, 0), (4, 1, 0, 1, 0), (5, 1, 3, 1, 1),
         (0, 0, 3, 0, 0), (6, 0, 3, 0, 0), (7, 0, 3, 0, 0), (0, 1, 3, 2, 0), (7, 1, 3, 2, 0),
         (6, 1, 3, 2, 0), (1, 1, 0, 2, 0), (4, 1, 0, 2, 0), (0, 1, 1, 0, 0), (7, 1, 1, 0, 0),
         (5, 1, 1, 0, 0), (0, 0, 2, 0, 0), (7, 0, 2, 0, 0), (6, 0, 2, 0, 0), (0, 0, 3, 0, 1),
         (7, 0, 3, 0, 1), (5, 0, 3, 0, 1), (6, 1, 1, 0, 0), (0, 0, 1, 0, 1), (7, 0, 1, 0, 1),
         (0, 1, 3, 2, 1), (7, 1, 3, 2, 1), (0, 0, 1, 1, 1), (7, 0, 1, 1, 1), (0, 1, 1, 2, 0),
         (7, 1, 1, 2, 0), (0, 0, 2, 1, 0), (6, 0, 2, 1, 0), (5, 0, 2, 1, 0), (7, 0, 2, 1, 0),
         (0, 0, 2, 0, 1), (5, 0, 2, 0, 1), (7, 0, 2, 0, 1), (6, 1, 1, 2, 0), (0, 0, 1, 2, 1),
         (7, 0, 1, 2, 1), (5, 1, 1, 2, 0), (0, 1, 1, 0, 1), (7, 1, 1, 0, 1), (0, 0, 1, 3, 1),
         (7, 0, 1, 3, 1),),
        ((5, 1, 3, 2, 0), (0, 1, 1, 1, 0), (7, 1, 1, 1, 0), (0, 1, 2, 3, 0), (6, 1, 2, 3, 0),
         (7, 1, 2, 3, 0), (0, 0, 2, 1, 1), (7, 0, 2, 1, 1), (0, 0, 2, 2, 0), (7, 0, 2, 2, 0),
         (6, 0, 2, 2, 0), (0, 1, 1, 2, 1), (7, 1, 1, 2, 1), (0, 0, 3, 1, 1), (7, 0, 3, 1, 1),
         (6, 0, 3, 1, 1), (0, 1, 1, 3, 0), (7, 1, 1, 3, 0), (0, 1, 2, 2, 0), (5, 1, 2, 2, 0),
         (7, 1, 2, 2, 0), (0, 1, 2, 3, 1), (7, 1, 2, 3, 1), (0, 0, 2, 3, 0), (7, 0, 2, 3, 0),
         (6, 0, 2, 3, 0), (5, 1, 2, 3, 1), (0, 0, 2, 2, 1), (7, 0, 2, 2, 1), (5, 0, 2, 2, 1),
         (0, 0, 3, 3, 0), (7, 0, 3, 3, 0), (6, 0, 3, 3, 0), (0, 1, 2, 1, 0), (7, 1, 2, 1, 0),
         (0, 0, 3, 1, 0), (7, 0, 3, 1, 0), (6, 1, 2, 2, 0), (1, 1, 0, 3, 0), (4, 1, 0, 3, 0),
         (5, 1, 3, 2, 1), (0, 0, 2, 3, 1), (7, 0, 2, 3, 1), (5, 0, 2, 3, 1),),
        ((0, 1, 2, 0, 0), (7, 1, 2, 0, 0), (6, 1, 2, 0, 0), (5, 1, 0, 0, 0), (0, 0, 3, 3, 1),
         (7, 0, 3, 3, 1), (0, 0, 3, 2, 1), (7, 0, 3, 2, 1),),
        ((0, 1, 2, 2, 1), (7, 1, 2, 2, 1), (0, 1, 3, 0, 0), (6, 1, 3, 0, 0), (7, 1, 3, 0, 0),
         (5, 1, 0, 1, 1), (0, 1, 2, 0, 1), (7, 1, 2, 0, 1), (5, 1, 2, 0, 1), (0, 1, 3, 3, 1),
         (7, 1, 3, 3, 1), (5, 1, 0, 3, 1), (0, 1, 3, 0, 1), (7, 1, 3, 0, 1),),
        ((0, 1, 2, 1, 1), (7, 1, 2, 1, 1),),
        ((5, 1, 0, 2, 0), (0, 1, 1, 1, 1), (7, 1, 1, 1, 1), (5, 1, 0, 2, 1), (0, 1, 1, 3, 1),
         (7, 1, 1, 3, 1),),
        (),
        (),
    ),
    (
        ((3, 0, 0, 0, 0),),
        ((3, 0, 0, 1, 0),),
        (),
        (),
        (),
        (),
        (),
        (),
        ((2, 1, 0, 0, 0),),
        (),
        (),
        (),
        (),
        (),
        (),
        (),
        ((3, 0, 0, 3, 0),),
        ((1, 0, 0, 0, 0), (4, 0, 0, 0, 0), (1, 0, 0, 1, 0), (4, 0, 0, 1, 0), (3, 0, 0, 2, 0),
         (1, 0, 0, 3, 0), (4, 0, 0, 3, 0), (3, 1, 0, 1, 0), (3, 1, 0, 2, 0), (3, 1, 0, 3, 0),
         (1, 1, 0, 0, 0), (4, 1, 0, 0, 0), (3, 1, 0, 0, 0),),
        (),
        (),
        (),
        (),
        (),
        (),
        (),
    ),
    (
        ((3, 0, 0, 0, 0),),
        ((2, 0, 0, 1, 0),),
        (),
        (),
        (),
        (),
        (),
        (),
        (),
        (),
        (),
        (),
        (),
        (),
        (),
        (),
        ((3, 0, 0, 1, 0), (2, 0, 0, 2, 0), (0, 0, 0, 0, 0), (6, 0, 0, 0, 0), (7, 0, 0, 0, 0),
         (3, 1, 0, 0, 0), (2, 0, 0, 3, 0), (0, 0, 0, 1, 1), (6, 0, 0, 1, 1), (7, 0, 0, 1, 1),
         (0, 0, 0, 0, 1), (7, 0, 0, 0, 1), (0, 0, 1, 0, 0), (6, 0, 1, 0, 0), (7, 0, 1, 0, 0),
         (3, 1, 0, 3, 0), (0, 0, 1, 3, 0), (6, 0, 1, 3, 0), (2, 1, 0, 1, 0), (7, 0, 1, 3, 0),
         (0, 0, 0, 1, 0), (7, 0, 0, 1, 0), (0, 0, 3, 2, 0), (7, 0, 3, 2, 0), (6, 0, 3, 2, 0),
         (0, 0, 1, 0, 1), (7, 0, 1, 0, 1), (0, 0, 1, 1, 0), (7, 0, 1, 1, 0), (6, 0, 1, 1, 0),
         (0, 0, 3, 0, 0), (5, 0, 3, 0, 0), (7, 0, 3, 0, 0), (0, 0, 1, 3, 1), (7, 0, 1, 3, 1),
         (0, 1, 1, 1, 0), (7, 1, 1, 1, 0), (0, 0, 0, 2, 1), (7, 0, 0, 2, 1), (6, 0, 0, 2, 1),
         (2, 1, 0, 2, 0), (0, 0, 3, 2, 1), (7, 0, 3, 2, 1), (0, 0, 1, 2, 0), (7, 0, 1, 2, 0),
         (6, 0, 1, 2, 0), (5, 0, 1, 0, 1), (0, 0, 3, 1, 0), (7, 0, 3, 1, 0), (0, 1, 1, 3, 0),
         (7, 1, 1, 3, 0), (0, 0, 1, 1, 1), (7, 0, 1, 1, 1), (6, 0, 3, 1, 0), (0, 0, 0, 3, 1),
         (7, 0, 0, 3, 1), (5, 0, 1, 1, 1), (0, 0, 0, 2, 0), (7, 0, 0, 2, 0), (6, 0, 0, 3, 1),
         (0, 1, 3, 3, 0), (7, 1, 3, 3, 0), (0, 0, 1, 2, 1), (7, 0, 1, 2, 1), (5, 0, 1, 2, 1),),
        ((6, 1, 3, 3, 0), (0, 1, 3, 1, 1), (7, 1, 3, 1, 1), (5, 0, 1, 3, 1), (0, 0, 3, 1, 1),
         (7, 0, 3, 1, 1), (0, 0, 3, 0, 1), (7, 0, 3, 0, 1), (0, 0, 3, 3, 0), (6, 0, 3, 3, 0),
         (7, 0, 3, 3, 0), (0, 0, 0, 3, 0), (7, 0, 0, 3, 0),),
        ((6, 1, 1, 1, 0), (0, 0, 2, 2, 0), (7, 0, 2, 2, 0), (5, 0, 2, 2, 0), (0, 1, 1, 0, 0),
         (7, 1, 1, 0, 0), (5, 0, 3, 1, 1), (0, 1, 3, 3, 1), (7, 1, 3, 3, 1), (0, 0, 2, 0, 1),
         (7, 0, 2, 0, 1), (6, 0, 2, 0, 1), (0, 0, 3, 3, 1), (7, 0, 3, 3, 1),),
        ((0, 0, 2, 3, 0), (7, 0, 2, 3, 0), (5, 0, 2, 3, 0), (0, 0, 2, 1, 0), (7, 0, 2, 1, 0),
         (6, 0, 2, 1, 0), (5, 0, 3, 3, 0), (0, 1, 1, 1, 1), (7, 1, 1, 1, 1), (6, 1, 1, 3, 0),
         (0, 1, 1, 2, 0), (7, 1, 1, 2, 0), (2, 1, 0, 3, 0), (0, 0, 2, 0, 0), (7, 0, 2, 0, 0),
         (0, 1, 3, 0, 0), (6, 1, 3, 0, 0), (7, 1, 3, 0, 0), (0, 1, 3, 2, 0), (7, 1, 3, 2, 0),
         (0, 0, 2, 1, 1), (7, 0, 2, 1, 1), (0, 1, 2, 0, 0), (7, 1, 2, 0, 0), (5, 1, 2, 0, 0),
         (0, 1, 2, 2, 0), (7, 1, 2, 2, 0), (6, 1, 2, 2, 0), (5, 0, 3, 2, 1), (0, 1, 1, 3, 1),
         (7, 1, 1, 3, 1), (6, 1, 3, 1, 1), (0, 0, 2, 2, 1), (7, 0, 2, 2, 1), (5, 1, 3, 0, 0),
         (0, 1, 3, 0, 1), (7, 1, 3, 0, 1), (0, 1, 2, 3, 1), (7, 1, 2, 3, 1), (5, 1, 3, 3, 1),
         (0, 1, 2, 2, 1), (7, 1, 2, 2, 1), (6, 1, 2, 3, 1), (0, 1, 2, 1, 0), (7, 1, 2, 1, 0),
         (6, 1, 2, 1, 0), (0, 0, 2, 3, 1), (7, 0, 2, 3, 1),),
        ((0, 1, 3, 1, 0), (7, 1, 3, 1, 0), (6, 1, 1, 0, 0), (0, 1, 3, 2, 1), (7, 1, 3, 2, 1),),
        ((5, 1, 1, 1, 1), (0, 1, 2, 1, 1), (7, 1, 2, 1, 1), (5, 1, 2, 1, 1), (6, 1, 1, 2, 0),
         (0, 1, 0, 0, 0), (7, 1, 0, 0, 0), (5, 1, 1, 3, 1), (0, 1, 2, 3, 0), (7, 1, 2, 3, 0),
         (6, 1, 0, 0, 0), (0, 1, 2, 0, 1), (7, 1, 2, 0, 1),),
        ((0, 1, 1, 0, 1), (7, 1, 1, 0, 1), (0, 1, 0, 1, 1), (7, 1, 0, 1, 1), (6, 1, 0, 1, 1),
         (0, 1, 1, 2, 1), (7, 1, 1, 2, 1),),
        ((0, 1, 0, 3, 1), (7, 1, 0, 3, 1), (6, 1, 0, 3, 1), (0, 1, 0, 0, 1), (7, 1, 0, 0, 1),
         (0, 1, 0, 2, 0), (7, 1, 0, 2, 0), (0, 1, 0, 1, 0), (7, 1, 0, 1, 0), (0, 1, 0, 2, 1),
         (7, 1, 0, 2, 1), (0, 1, 0, 3, 0), (7, 1, 0, 3, 0),),
        (),
    ),
    (
        ((2, 0, 0, 0, 0),),
        (),
        ((3, 0, 0, 2, 0),),
        (),
        (),
        (),
        (),
        (),
        (),
        (),
        (),
        (),
        (),
        (),
        (),
        (),
        ((2, 0, 0, 1, 0), (3, 1, 0, 1, 0), (2, 0, 0, 3, 0), (3, 1, 0, 3, 0), (2, 1, 0, 0, 0),
         (1, 1, 0, 0, 0), (4, 1, 0, 0, 0), (3, 1, 0, 2, 0),),
        (),
        (),
        (),
        (),
        (),
        (),
        (),
        (),
    ),
    (
        ((3, 0, 1, 0, 0),),
        (),
        (),
        ((2, 0, 1, 3, 0),),
        (),
        (),
        (),
        (),
        (),
        (),
        (),
        (),
        (),
        (),
        (),
        (),
        ((3, 0, 1, 1, 0), (2, 1, 1, 1, 0),),
        ((1, 0, 1, 0, 0), (4, 0, 1, 0, 0), (3, 0, 1, 2, 0), (2, 1, 1, 3, 0), (3, 0, 1, 3, 0),
         (3, 1, 1, 0, 0), (3, 1, 1, 2, 0), (3, 1, 1, 1, 0), (1, 0, 1, 1, 0), (4, 0, 1, 1, 0),
         (3, 1, 1, 3, 0), (1, 0, 1, 2, 0), (4, 0, 1, 2, 0),),
        (),
        ((1, 1, 1, 3, 0), (4, 1, 1, 3, 0), (1, 1, 1, 1, 0), (4, 1, 1, 1, 0), (1, 1, 1, 2, 0),
         (4, 1, 1, 2, 0),),
        ((1, 1, 1, 0, 0), (4, 1, 1, 0, 0),),
        (),
        (),
        (),
        (),
    ),
    (
        ((5, 0, 1, 0, 0), (7, 0, 1, 0, 0),),
        (),
        (),
        (),
        (),
        ((7, 0, 1, 0, 1),),
        (),
        (),
        (),
        (),
        ((7, 0, 1, 1, 0),),
        (),
        (),
        (),
        (),
        ((7, 0, 1, 1, 1),),
        ((5, 0, 1, 1, 0), (7, 0, 1, 2, 0), (7, 0, 1, 2, 1), (7, 0, 1, 3, 0), (7, 0, 1, 3, 1),
         (7, 1, 1, 0, 0),),
        ((7, 1, 1, 0, 1), (0, 0, 0, 0, 0), (6, 0, 0, 0, 0), (7, 0, 0, 0, 0), (7, 1, 1, 1, 0),
         (7, 1, 1, 1, 1), (7, 1, 1, 2, 0), (7, 1, 1, 2, 1), (7, 1, 1, 3, 0), (0, 0, 0, 1, 0),
         (6, 0, 0, 1, 0), (7, 0, 0, 1, 0), (5, 0, 1, 2, 1), (1, 0, 1, 2, 0), (4, 0, 1, 2, 0),
         (7, 1, 1, 3, 1), (0, 0, 3, 0, 0), (6, 0, 3, 0, 0), (7, 0, 3, 0, 0), (0, 0, 0, 0, 1),
         (7, 0, 0, 0, 1), (0, 0, 0, 1, 1), (7, 0, 0, 1, 1), (0, 0, 0, 3, 0), (7, 0, 0, 3, 0),
         (0, 0, 3, 1, 0), (6, 0, 3, 1, 0), (7, 0, 3, 1, 0), (0, 0, 3, 0, 1), (7, 0, 3, 0, 1),
         (5, 0, 3, 0, 1), (5, 0, 0, 3, 0), (0, 0, 3, 1, 1), (7, 0, 3, 1, 1), (5, 0, 1, 3, 0),
         (0, 1, 3, 0, 0), (6, 1, 3, 0, 0), (7, 1, 3, 0, 0), (5, 0, 0, 0, 0), (0, 1, 3, 0, 1),
         (7, 1, 3, 0, 1), (5, 0, 0, 1, 1), (0, 1, 3, 3, 0), (6, 1, 3, 3, 0), (7, 1, 3, 3, 0),
         (0, 0, 0, 2, 0), (6, 0, 0, 2, 0), (7, 0, 0, 2, 0), (5, 0, 0, 2, 0), (0, 1, 3, 3, 1),
         (7, 1, 3, 3, 1), (0, 0, 2, 0, 0), (7, 0, 2, 0, 0), (0, 0, 3, 2, 0), (6, 0, 3, 2, 0),
         (7, 0, 3, 2, 0), (1, 0, 1, 3, 0), (4, 0, 1, 3, 0), (0, 0, 0, 2, 1), (7, 0, 0, 2, 1),
         (5, 0, 0, 2, 1), (0, 0, 3, 2, 1), (7, 0, 3, 2, 1), (5, 0, 3, 2, 1), (0, 0, 3, 3, 0),
         (6, 0, 3, 3, 0), (7, 0, 3, 3, 0), (0, 0, 2, 3, 0), (7, 0, 2, 3, 0), (1, 1, 1, 0, 0),
         (4, 1, 1, 0, 0), (0, 1, 0, 1, 0), (7, 1, 0, 1, 0), (6, 1, 0, 1, 0), (5, 0, 2, 3, 0),
         (0, 0, 3, 3, 1), (7, 0, 3, 3, 1), (5, 0, 3, 3, 1),),
        ((0, 0, 2, 2, 0), (7, 0, 2, 2, 0), (6, 0, 2, 2, 0), (0, 1, 0, 2, 0), (6, 1, 0, 2, 0),
         (5, 1, 0, 1, 0), (0, 0, 0, 3, 1), (7, 0, 0, 3, 1),),
        ((7, 1, 0, 2, 0), (0, 1, 0, 1, 1), (7, 1, 0, 1, 1), (0, 1, 0, 3, 0), (7, 1, 0, 3, 0),
         (5, 1, 0, 3, 0), (0, 1, 3, 2, 0), (7, 1, 3, 2, 0), (0, 1, 0, 2, 1), (7, 1, 0, 2, 1),
         (1, 1, 1, 1, 0), (4, 1, 1, 1, 0), (6, 1, 0, 3, 0), (0, 1, 2, 0, 0), (7, 1, 2, 0, 0),
         (0, 0, 2, 1, 0), (6, 0, 2, 1, 0), (5, 1, 3, 0, 1), (7, 0, 2, 1, 0), (0, 0, 2, 2, 1),
         (7, 0, 2, 2, 1), (6, 1, 2, 0, 0), (0, 1, 0, 0, 0), (7, 1, 0, 0, 0), (5, 1, 0, 2, 0),
         (0, 0, 2, 0, 1), (7, 0, 2, 0, 1), (0, 0, 2, 1, 1), (7, 0, 2, 1, 1), (0, 1, 2, 2, 0),
         (7, 1, 2, 2, 0), (0, 1, 3, 1, 1), (6, 1, 3, 1, 1), (5, 1, 0, 2, 1), (7, 1, 3, 1, 1),
         (0, 1, 0, 3, 1), (7, 1, 0, 3, 1), (6, 1, 3, 2, 0), (0, 1, 0, 0, 1), (7, 1, 0, 0, 1),
         (5, 1, 1, 0, 0), (0, 1, 2, 0, 1), (7, 1, 2, 0, 1), (0, 0, 2, 3, 1), (7, 0, 2, 3, 1),),
        ((5, 1, 1, 1, 1),),
        ((0, 1, 3, 1, 0), (7, 1, 3, 1, 0), (0, 1, 2, 3, 0), (7, 1, 2, 3, 0), (6, 1, 2, 3, 0),
         (5, 1, 1, 2, 1), (0, 1, 3, 2, 1), (7, 1, 3, 2, 1),),
        ((5, 1, 2, 0, 1), (0, 1, 2, 3, 1), (7, 1, 2, 3, 1), (0, 1, 2, 1, 0), (6, 1, 2, 1, 0),
         (7, 1, 2, 1, 0), (5, 1, 2, 3, 1), (5, 1, 1, 3, 0), (0, 1, 2, 1, 1), (7, 1, 2, 1, 1),
         (5, 1, 1, 3, 1), (0, 1, 2, 2, 1), (7, 1, 2, 2, 1),),
        (),
        (),
    ),
    (
        ((2, 0, 1, 0, 0), (3, 0, 1, 0, 0),),
        (),
        (),
        (),
        (),
        (),
        (),
        (),
        (),
        (),
        (),
        (),
        (),
        (),
        (),
        (),
        ((2, 0, 1, 1, 0), (2, 0, 1, 2, 0), (1, 0, 1, 3, 0), (4, 0, 1, 3, 0), (2, 1, 1, 3, 0),
         (1, 1, 1, 1, 0), (4, 1, 1, 1, 0), (2, 1, 1, 1, 0), (1, 1, 1, 3, 0), (4, 1, 1, 3, 0),
         (2, 1, 1, 2, 0), (3, 0, 1, 3, 0), (2, 1, 1, 0, 0), (3, 0, 1, 2, 0),),
        ((3, 1, 1, 0, 0),),
        ((3, 1, 1, 2, 0),),
        (),
        (),
        (),
        (),
        (),
        (),
    ),
    (
        ((3, 0, 1, 0, 0),),
        (),
        ((2, 0, 1, 2, 0),),
        (),
        (),
        (),
        (),
        (),
        (),
        (),
        (),
        (),
        (),
        (),
        (),
        (),
        ((2, 0, 1, 3, 0), (0, 0, 1, 0, 0), (6, 0, 1, 0, 0), (7, 0, 1, 0, 0), (2, 1, 1, 0, 0),
         (0, 0, 1, 0, 1), (7, 0, 1, 0, 1), (0, 0, 1, 1, 0), (6, 0, 1, 1, 0), (7, 0, 1, 1, 0),
         (2, 1, 1, 1, 0), (0, 0, 3, 1, 0), (7, 0, 3, 1, 0), (6, 0, 3, 1, 0), (0, 0, 1, 1, 1),
         (7, 0, 1, 1, 1), (0, 0, 1, 2, 1), (6, 0, 1, 2, 1), (7, 0, 1, 2, 1), (0, 0, 3, 1, 1),
         (7, 0, 3, 1, 1), (0, 0, 3, 2, 0), (7, 0, 3, 2, 0), (5, 0, 3, 2, 0), (0, 0, 3, 0, 1),
         (6, 0, 3, 0, 1), (7, 0, 3, 0, 1), (0, 0, 1, 2, 0), (7, 0, 1, 2, 0), (0, 0, 0, 3, 0),
         (6, 0, 0, 3, 0), (7, 0, 0, 3, 0), (0, 1, 0, 0, 0), (6, 1, 0, 0, 0), (3, 0, 1, 1, 0),
         (7, 1, 0, 0, 0), (0, 0, 3, 0, 0), (7, 0, 3, 0, 0), (0, 0, 3, 3, 0), (7, 0, 3, 3, 0),
         (5, 0, 3, 3, 0), (0, 0, 1, 3, 0), (7, 0, 1, 3, 0), (6, 0, 1, 3, 0), (0, 0, 0, 3, 1),
         (7, 0, 0, 3, 1), (0, 0, 0, 0, 0), (7, 0, 0, 0, 0), (6, 0, 0, 0, 0), (3, 1, 1, 3, 0),
         (5, 0, 0, 3, 1), (0, 1, 0, 0, 1), (7, 1, 0, 0, 1), (0, 1, 3, 1, 0), (7, 1, 3, 1, 0),
         (0, 0, 0, 1, 1), (7, 0, 0, 1, 1), (6, 0, 0, 1, 1), (0, 0, 1, 3, 1), (7, 0, 1, 3, 1),),
        ((0, 0, 0, 2, 0), (7, 0, 0, 2, 0), (0, 0, 2, 0, 0), (6, 0, 2, 0, 0), (3, 1, 1, 2, 0),
         (7, 0, 2, 0, 0), (0, 0, 0, 0, 1), (7, 0, 0, 0, 1), (6, 1, 3, 1, 0), (0, 1, 3, 2, 0),
         (7, 1, 3, 2, 0), (5, 1, 3, 2, 0), (0, 0, 0, 2, 1), (7, 0, 0, 2, 1), (0, 0, 0, 1, 0),
         (7, 0, 0, 1, 0),),
        ((0, 0, 3, 2, 1), (7, 0, 3, 2, 1), (3, 1, 1, 1, 0), (0, 0, 2, 1, 0), (7, 0, 2, 1, 0),
         (5, 0, 2, 1, 0), (6, 0, 2, 1, 0), (0, 0, 2, 0, 1), (7, 0, 2, 0, 1), (5, 0, 2, 0, 1),
         (6, 1, 3, 2, 0), (0, 0, 3, 3, 1), (7, 0, 3, 3, 1),),
        ((0, 1, 3, 1, 1), (7, 1, 3, 1, 1), (5, 1, 3, 1, 1), (0, 0, 2, 3, 0), (7, 0, 2, 3, 0),
         (6, 0, 2, 3, 0), (5, 1, 0, 0, 1), (0, 0, 2, 1, 1), (7, 0, 2, 1, 1), (0, 1, 0, 1, 0),
         (7, 1, 0, 1, 0), (0, 0, 2, 2, 0), (7, 0, 2, 2, 0), (6, 0, 2, 2, 0), (0, 1, 3, 2, 1),
         (7, 1, 3, 2, 1), (6, 1, 0, 1, 0), (0, 1, 0, 3, 0), (7, 1, 0, 3, 0), (0, 0, 2, 3, 1),
         (7, 0, 2, 3, 1), (5, 0, 2, 3, 1), (6, 1, 0, 3, 0), (0, 1, 3, 0, 1), (7, 1, 3, 0, 1),
         (0, 1, 2, 3, 0), (7, 1, 2, 3, 0), (5, 1, 2, 3, 0), (0, 0, 2, 2, 1), (7, 0, 2, 2, 1),),
        ((6, 1, 3, 0, 1), (0, 1, 0, 2, 0), (7, 1, 0, 2, 0), (0, 1, 0, 1, 1), (7, 1, 0, 1, 1),
         (0, 1, 3, 3, 0), (7, 1, 3, 3, 0), (6, 1, 3, 3, 0), (0, 1, 0, 2, 1), (7, 1, 0, 2, 1),
         (0, 1, 2, 1, 0), (5, 1, 2, 1, 0), (7, 1, 2, 1, 0), (0, 1, 0, 3, 1), (7, 1, 0, 3, 1),),
        ((0, 1, 1, 0, 0), (7, 1, 1, 0, 0), (0, 1, 2, 2, 0), (7, 1, 2, 2, 0), (6, 1, 2, 2, 0),
         (0, 1, 3, 0, 0), (7, 1, 3, 0, 0), (6, 1, 2, 1, 0), (0, 1, 1, 1, 1), (7, 1, 1, 1, 1),
         (0, 1, 2, 0, 0), (7, 1, 2, 0, 0), (0, 1, 3, 3, 1), (7, 1, 3, 3, 1),),
        ((6, 1, 1, 0, 0), (0, 1, 1, 2, 1), (7, 1, 1, 2, 1), (0, 1, 2, 2, 1), (5, 1, 2, 2, 1),
         (7, 1, 2, 2, 1), (6, 1, 1, 1, 1), (0, 1, 2, 0, 1), (7, 1, 2, 0, 1), (0, 1, 2, 1, 1),
         (7, 1, 2, 1, 1), (6, 1, 1, 2, 1), (0, 1, 2, 3, 1), (7, 1, 2, 3, 1),),
        ((0, 1, 1, 0, 1), (7, 1, 1, 0, 1), (0, 1, 1, 3, 0), (7, 1, 1, 3, 0), (0, 1, 1, 1, 0),
         (7, 1, 1, 1, 0), (0, 1, 1, 3, 1), (7, 1, 1, 3, 1), (0, 1, 1, 2, 0), (7, 1, 1, 2, 0),),
        (),
    ),
)


def local_plain(tokens, norm_gain, up_trained, down_trained):
    shards = lax.axis_size("fs")
    groups = lax.axis_size("tp")
    rows_local = up_trained.shape[0]
    cols_local = up_trained.shape[1]
    folded = (norm_gain[:, None] * up_trained).astype(jnp.bfloat16)
    stacked = jnp.stack([folded, down_trained.astype(jnp.bfloat16)])
    served_width = cols_local * groups // shards
    blocks_here = cols_local // served_width
    quarter_rows = rows_local // groups
    pieces = stacked.reshape(2, groups, quarter_rows, blocks_here, served_width)
    moved = lax.all_to_all(pieces, "tp", split_axis=1, concat_axis=3, tiled=True)
    placed = lax.all_to_all(moved, "fs", split_axis=3, concat_axis=2, tiled=True)
    ordered = placed.reshape(2, shards, quarter_rows, served_width)
    joined = lax.all_gather(ordered, "tp", axis=2, tiled=True)
    owned = joined.reshape(2, rows_local * shards, served_width)
    up_serving = owned[0]
    down_serving = owned[1]
    values = tokens.astype(jnp.float32)
    scale = lax.rsqrt(jnp.mean(values * values, axis=1, keepdims=True) + epsilon)
    normed = (values * scale).astype(jnp.bfloat16)
    hidden = jnp.dot(normed, up_serving, preferred_element_type=jnp.float32)
    active = jnp.square(jax.nn.relu(hidden)).astype(jnp.bfloat16)
    summed = lax.psum_scatter(
        lax.dot_general(
            down_serving, active, (((1,), (1,)), ((), ())), preferred_element_type=jnp.float32
        ),
        "fs",
        scatter_dimension=0,
        tiled=True,
    )
    prompt_output = summed.T.astype(jnp.bfloat16)
    return (up_serving, down_serving, prompt_output)


def kernel(
    tokens_hbm, gain_hbm, up_hbm, down_hbm, whole, prompt_out,
    raw, gain_rows, gain, cast, relay, toks, normed, hidden, active, rs_send, rs_recv, rs_own,
    in_sem, misc_sem, got_sem, relay_sem, block_sem, src_sem, out_sem, rs_ssem, rs_rsem,
):
    y = lax.axis_index("grp")
    z = lax.axis_index("fs")
    t = lax.axis_index("tp")
    mirrored = z // 2
    role = jnp.where(mirrored == 1, 4 * (3 - z) + (3 - t), 4 * z + t)
    is_own = z == t
    is_active = t % 2 == z % 2
    t_x = jnp.where(t < 2, t + 2, t - 2)
    t_c = t + 1 - 2 * (t % 2)
    to_x = {"tp": t_x}
    to_c = {"tp": t_c}
    to_y = {"grp": 1 - y}
    rows_local, width = cast.shape[1], cast.shape[2]
    size = rows_local // (2 * PAIRS)
    trained = (up_hbm, down_hbm)
    planes = [jnp.where(mirrored == 1, 3 - k, k) for k in range(4)]
    sides = [y, 1 - y]

    def part(pair, side):
        return 2 * pair + sides[side]

    def ds(start, extent):
        return pl.ds(pl.multiple_of(start, extent), extent)

    def local_rows(pair, side):
        return ds(part(pair, side) * size, size)

    def unit(m, plane, pair, side):
        return whole.at[m, ds(plane * rows_local + part(pair, side) * size, size)]

    def remote(src, dst, ssem, rsem, where):
        return pltpu.make_async_remote_copy(
            src_ref=src, dst_ref=dst, send_sem=ssem, recv_sem=rsem,
            device_id=where, device_id_type=MESH,
        )

    def fetch(m, pair, side):
        rows = local_rows(pair, side)
        return pltpu.make_async_copy(
            trained[m].at[rows], raw.at[m, rows], in_sem.at[m, 2 * pair + side]
        )

    get_gain = pltpu.make_async_copy(gain_hbm, gain_rows, misc_sem.at[0])
    get_toks = pltpu.make_async_copy(tokens_hbm, toks, misc_sem.at[1])
    get_gain.start()
    for pair in range(PAIRS):
        fetch(0, pair, 0).start()

    barrier = pltpu.get_barrier_semaphore()
    others = [{"fs": lax.rem(z + k, 4)} for k in range(1, 4)]
    for where in [to_x, to_c, to_y] + others:
        pl.semaphore_signal(barrier, inc=1, device_id=where, device_id_type=MESH)

    get_gain.wait()
    lanes = gain_rows.shape[1]
    for q in range(gain_rows.shape[0]):
        square = (lanes, lanes)
        chosen = jnp.where(
            lax.broadcasted_iota(jnp.int32, square, 0) == lax.broadcasted_iota(jnp.int32, square, 1),
            jnp.broadcast_to(gain_rows[pl.ds(q, 1), :], square), 0.0,
        )
        column = jnp.sum(chosen, axis=1, keepdims=True)
        gain[pl.ds(q * lanes, lanes), :] = jnp.broadcast_to(column, square)

    piece = 16

    def cast_unit(m, pair, side):
        fetch(m, pair, side).wait()
        base = part(pair, side) * size

        def store(into, shift):
            @pl.loop(0, size // piece)
            def _(i):
                here = ds(base + i * piece, piece)
                there = ds(shift + base + i * piece, piece)
                if m == 0:
                    factor = gain[here, :]
                    for j in range(width // lanes):
                        cols = pl.ds(j * lanes, lanes)
                        into[0, there, cols] = (raw[0, here, cols] * factor).astype(jnp.bfloat16)
                else:
                    into[m, there, :] = raw[m, here, :].astype(jnp.bfloat16)

        @pl.when(is_own)
        def _():
            store(whole, z * rows_local)

        if side == 0:
            @pl.when(jnp.logical_not(is_own))
            def _():
                store(cast, 0)

    def step(kind, m, k, pair, side):
        plane = planes[k]
        place = part(pair, side)
        if kind == GET:
            here = unit(m, plane, pair, side)
            remote(here, here, out_sem.at[0, m], got_sem.at[m, plane, place], to_x).wait_recv()
        elif kind == GET_RELAY:
            here = relay.at[m, ds(place * size, size)]
            remote(here, here, src_sem.at[m], relay_sem.at[m, place], to_x).wait_recv()
        elif kind == SWAP:
            remote(
                cast.at[m, local_rows(pair, side)], relay.at[m, ds(place * size, size)],
                src_sem.at[m], relay_sem.at[m, place], to_x,
            ).start()
        elif kind in (HOP, HOP_RELAY):
            src = (cast if kind == HOP else relay).at[m, ds(place * size, size)]
            remote(
                src, unit(m, z, pair, side), src_sem.at[m], got_sem.at[m, z, place],
                {"fs": t if kind == HOP else t_x},
            ).start()
        elif kind == SEND_CORE:
            here = unit(m, plane, pair, side)
            remote(here, here, out_sem.at[2, m], block_sem.at[m, plane], to_c).start()
        else:
            here = unit(m, plane, pair, side)
            i = kind - SEND_X
            remote(
                here, here, out_sem.at[i, m], got_sem.at[m, plane, place], (to_x, to_y)[i]
            ).start()

    def run(segment):
        for r in range(8):
            if SCHEDULE[r][segment]:
                @pl.when(role == r)
                def _():
                    for s in SCHEDULE[r][segment]:
                        step(*s)

    casts = [(m, pair, side) for m in range(2) for side in range(2) for pair in range(PAIRS)]
    segment = 0
    for m, pair, side in casts:
        if side == 1:
            pl.when(is_own)(lambda: cast_unit(m, pair, side))
        else:
            cast_unit(m, pair, side)
        if segment == 0:
            @pl.when(is_own)
            def _():
                for p in range(PAIRS):
                    fetch(0, p, 1).start()
            for p in range(PAIRS):
                fetch(1, p, 0).start()
            @pl.when(is_own)
            def _():
                for p in range(PAIRS):
                    fetch(1, p, 1).start()
            get_toks.start()
            pl.semaphore_wait(barrier, 6)
        run(segment)
        segment += 1

    get_toks.wait()
    tokens_here = toks.shape[0]

    @pl.loop(0, tokens_here // piece)
    def _(i):
        here = ds(i * piece, piece)
        values = toks[here, :].astype(jnp.float32)
        scale = lax.rsqrt(jnp.mean(values * values, axis=1, keepdims=True) + epsilon)
        normed[here, :] = (values * scale).astype(jnp.bfloat16)

    def pick(table):
        chosen = planes[table[0]]
        for r in range(1, 8):
            if table[r] != table[0]:
                chosen = jnp.where(role == r, planes[table[r]], chosen)
        return chosen

    def listen(m, plane):
        @pl.when(jnp.logical_not(is_active))
        def _():
            here = whole.at[m, ds(plane * rows_local, rows_local)]
            remote(here, here, out_sem.at[2, m], block_sem.at[m, plane], to_c).wait_recv()

    tile = 512 if width % 512 == 0 else width

    def compute_up(k):
        plane = pick(ORDER[0][k])
        listen(0, plane)
        rows = ds(plane * rows_local, rows_local)

        @pl.loop(0, width // tile)
        def _(n):
            cols = ds(n * tile, tile)
            product = jnp.dot(
                normed[:, rows], whole[0, rows, cols], preferred_element_type=jnp.float32
            )
            if k > 0:
                product = product + hidden[:, cols]
            if k < 3:
                hidden[:, cols] = product
            else:
                active[:, cols] = jnp.square(jnp.maximum(product, 0.0)).astype(jnp.bfloat16)

    d_tile = 256 if rows_local % 256 == 0 else rows_local

    def scatter(k, plane):
        slot = lax.rem(z - plane + 3, 4)
        return remote(
            rs_send.at[k], rs_recv.at[slot], rs_ssem.at[k], rs_rsem.at[slot], {"fs": plane}
        )

    def compute_down(k):
        plane = pick(ORDER[1][k])
        listen(1, plane)

        @pl.loop(0, rows_local // d_tile)
        def _(n):
            cols = ds(n * d_tile, d_tile)
            product = lax.dot_general(
                active[...], whole[1, ds(plane * rows_local + n * d_tile, d_tile), :],
                (((1,), (1,)), ((), ())), preferred_element_type=jnp.float32,
            )
            if k < 3:
                rs_send[k, :, cols] = product.astype(jnp.bfloat16)
            else:
                rs_own[:, cols] = product
        if k < 3:
            scatter(k, plane).start()

    for m in range(2):
        for k in range(4):
            run(segment)
            segment += 1
            (compute_up, compute_down)[m](k)
    run(segment)

    for k in range(3):
        here = rs_recv.at[k]
        remote(here, here, rs_ssem.at[k], rs_rsem.at[k], {"fs": lax.rem(z + 1, 4)}).wait_recv()

    @pl.loop(0, tokens_here // piece)
    def _(i):
        here = ds(i * piece, piece)
        total = rs_own[here, :]
        for k in range(3):
            total = total + rs_recv[k, here, :].astype(jnp.float32)
        prompt_out[here, :] = total.astype(prompt_out.dtype)

    def drain(sem, m, count):
        sent = whole.at[m, pl.ds(0, count * size)]
        remote(sent, sent, sem, got_sem.at[0, 0, 0], to_x).wait_send()

    for r in range(8):
        @pl.when(role == r)
        def _():
            for m in range(2):
                steps = [s for part_of in SCHEDULE[r] for s in part_of if s[1] == m]
                hops = sum(s[0] in (SWAP, HOP, HOP_RELAY) for s in steps)
                if hops:
                    drain(src_sem.at[m], m, hops)
                for i, kind in enumerate((SEND_X, SEND_Y, SEND_CORE)):
                    sends = sum(s[0] == kind for s in steps)
                    if sends:
                        drain(out_sem.at[i, m], m, sends)
    for k in range(3):
        here = rs_send.at[k]
        remote(here, here, rs_ssem.at[k], rs_rsem.at[k], {"fs": lax.rem(z + 1, 4)}).wait_send()


pieces_out = 8


def deliver(whole, prompt, up_out, down_out, prompt_out, sems, last):
    rows = whole.shape[1] // pieces_out
    copies = [
        pltpu.make_async_copy(
            whole.at[m, pl.ds(i * rows, rows)], out.at[pl.ds(i * rows, rows)], sems.at[m, i]
        )
        for m, out in enumerate((up_out, down_out))
        for i in range(pieces_out)
    ]
    copies.append(pltpu.make_async_copy(prompt, prompt_out, last))
    for copy in copies:
        copy.start()
    for copy in copies:
        copy.wait()


def local_kernel(tokens, norm_gain, up_trained, down_trained):
    shards = lax.axis_size("fs")
    rows_local, width = up_trained.shape
    tokens_here, features = tokens.shape
    any_space = pl.BlockSpec(memory_space=pl.ANY)
    dma = pltpu.SemaphoreType.DMA
    bf16, f32 = jnp.bfloat16, jnp.float32
    whole, prompt = pl.pallas_call(
        kernel,
        out_shape=(
            pltpu.VMEM((2, rows_local * shards, width), bf16),
            pltpu.VMEM((tokens_here, rows_local), bf16),
        ),
        in_specs=[any_space] * 4,
        out_specs=(pl.BlockSpec(memory_space=pltpu.VMEM),) * 2,
        scratch_shapes=[
            pltpu.VMEM((2, rows_local, width), f32),
            pltpu.VMEM((rows_local // 128, 128), f32),
            pltpu.VMEM((rows_local, 128), f32),
            pltpu.VMEM((2, rows_local, width), bf16),
            pltpu.VMEM((2, rows_local, width), bf16),
            pltpu.VMEM((tokens_here, features), bf16),
            pltpu.VMEM((tokens_here, features), bf16),
            pltpu.VMEM((tokens_here, width), f32),
            pltpu.VMEM((tokens_here, width), bf16),
            pltpu.VMEM((3, tokens_here, rows_local), bf16),
            pltpu.VMEM((3, tokens_here, rows_local), bf16),
            pltpu.VMEM((tokens_here, rows_local), f32),
            dma((2, 2 * PAIRS)), dma((2,)),
            dma((2, 4, 2 * PAIRS)), dma((2, 2 * PAIRS)), dma((2, 4)),
            dma((2,)), dma((3, 2)), dma((3,)), dma((3,)),
        ],
        compiler_params=pltpu.CompilerParams(
            collective_id=0, has_side_effects=True, vmem_limit_bytes=40 * 1024 * 1024
        ),
    )(tokens, norm_gain.reshape(rows_local // 128, 128), up_trained, down_trained)
    held = pl.BlockSpec(memory_space=pltpu.VMEM)
    return tuple(pl.pallas_call(
        deliver,
        out_shape=(
            jax.ShapeDtypeStruct((rows_local * shards, width), bf16),
            jax.ShapeDtypeStruct((rows_local * shards, width), bf16),
            jax.ShapeDtypeStruct((tokens_here, rows_local), bf16),
        ),
        in_specs=[held, held],
        out_specs=(any_space,) * 3,
        scratch_shapes=[dma((2, pieces_out)), dma(())],
        compiler_params=pltpu.CompilerParams(vmem_limit_bytes=8 * 1024 * 1024),
    )(whole, prompt))


def solution(mesh):
    in_specs = (P(("grp", "tp"), None), P("fs"), P("fs", "tp"), P("fs", "tp"))
    out_specs = (P("grp", "fs"), P("grp", "fs"), P(("grp", "tp"), "fs"))
    sizes = mesh.shape
    square = sizes["grp"] == 2 and sizes["fs"] == 4 and sizes["tp"] == 4
    local = local_kernel if square else local_plain
    return jax.shard_map(local, mesh=mesh, in_specs=in_specs, out_specs=out_specs, check_vma=False)
```

time: 122 us -> 99.4 us (0.81)
  the two profiles are of different devices: /device:TPU:1 before, /device:TPU:3 now
where the time goes in v3:
time: 99.4 us; the launch traced here: 98.5 us
  Pallas kernels  97.9 us (98%)
    pallas_call x1, Pallas kernels, local_kernel(): pl.pallas_call(kernel, out_shape=(pltpu.VMEM((2, rows_local * shards, wid...  91.9 us
    pallas_call x1, Pallas kernels, local_kernel(): pl.pallas_call(deliver, out_shape=(jax.ShapeDtypeStruct((rows_local * sha...  5.99 us

profile of v3, /device:TPU:3, one launch (start us, length us, event | category | flops | bytes accessed | tf_op | source)
XLA Modules:
  0.0 98.5 jit_solution(16578423130468153387)
XLA Ops:
  0.6 91.9 %shard_map.67 = (bf16[2,2048,2048]{2,1,0:T(8,128)(2,1)S(1)}, bf16[192,512]{1,0:T(8,128)(2,1)S(1)}) custom-call(bf16[192,2048]{1,0:T(8,128)(2,1)} %tokens_hbm.1, f32[4,128]{1,0:T(4,128)} %bitcast.1, f32[512,2048]{1,0:T(8,128)} %up_hbm.1, f32[512,2048]{1,0:T(8,128)} %down_hbm.1), custom_call_target="tpu_custom_call" | custom-call | tf_op jit(solution)/shard_map/pallas_call | solution.py:697
  92.5 6.0 %shard_map.68 = (bf16[2048,2048]{1,0:T(8,128)(2,1)}, bf16[2048,2048]{1,0:T(8,128)(2,1)}, bf16[192,512]{1,0:T(8,128)(2,1)}) custom-call(bf16[2,2048,2048]{2,1,0:T(8,128)(2,1)S(1)} %get-tuple-element.5.whole, bf16[192,512]{1,0:T(8,128)(2,1)S(1)} %get-tuple-element.6.prompt), custom_call_target="tpu_custom_call" | custom-call | tf_op jit(solution)/shard_map/pallas_call | solution.py:727

commit v4 on v3

v4 whole, which is shorter than its diff:
```python
import jax
import jax.numpy as jnp
from jax import lax
from jax.experimental import pallas as pl
from jax.experimental.pallas import tpu as pltpu
from jax.sharding import PartitionSpec as P

epsilon = 1e-06
MESH = pl.DeviceIdType.MESH

GET, GET_RELAY, SWAP, HOP, HOP_RELAY, SEND_X, SEND_Y, SEND_CORE = range(8)
PAIRS = 4
ORDER = (
    (
        (0, 0, 0, 0, 1, 1, 3, 3),
        (3, 3, 3, 3, 3, 3, 1, 1),
        (1, 1, 1, 1, 0, 0, 0, 0),
        (2, 2, 2, 2, 2, 2, 2, 2),
    ),
    (
        (1, 1, 1, 1, 3, 3, 3, 3),
        (2, 2, 3, 3, 0, 0, 2, 2),
        (3, 3, 2, 2, 2, 2, 0, 0),
        (0, 0, 0, 0, 1, 1, 1, 1),
    ),
)
SCHEDULE = (
    (
        ((5, 0, 0, 0, 0), (7, 0, 0, 0, 0),),
        ((5, 0, 0, 1, 0),),
        (),
        (),
        (),
        ((7, 0, 0, 0, 1),),
        (),
        ((5, 0, 0, 2, 0),),
        (),
        (),
        ((7, 0, 0, 1, 0),),
        (),
        (),
        (),
        (),
        ((7, 0, 0, 1, 1),),
        ((7, 0, 0, 2, 0), (7, 0, 0, 2, 1), (7, 0, 0, 3, 0), (7, 0, 0, 3, 1), (7, 1, 0, 0, 0),),
        ((7, 1, 0, 0, 1), (7, 1, 0, 1, 0), (7, 1, 0, 1, 1), (7, 1, 0, 2, 0), (7, 1, 0, 2, 1),
         (7, 1, 0, 3, 0), (5, 0, 0, 3, 0), (7, 1, 0, 3, 1), (1, 0, 0, 0, 0), (4, 0, 0, 0, 0),
         (0, 0, 1, 0, 0), (7, 0, 1, 0, 0), (5, 0, 1, 0, 0), (0, 0, 3, 0, 0), (6, 0, 3, 0, 0),
         (7, 0, 3, 0, 0), (5, 1, 0, 0, 1), (0, 0, 3, 0, 1), (7, 0, 3, 0, 1), (1, 0, 0, 1, 0),
         (4, 0, 0, 1, 0), (0, 0, 1, 2, 0), (7, 0, 1, 2, 0), (5, 0, 1, 2, 0), (0, 0, 3, 2, 0),
         (6, 0, 3, 2, 0), (7, 0, 3, 2, 0), (0, 0, 3, 2, 1), (7, 0, 3, 2, 1), (5, 0, 3, 2, 1),
         (1, 0, 0, 3, 0), (4, 0, 0, 3, 0), (0, 0, 1, 3, 0), (6, 0, 1, 3, 0), (7, 0, 1, 3, 0),
         (0, 0, 3, 3, 0), (7, 0, 3, 3, 0), (6, 0, 3, 3, 0), (5, 0, 3, 3, 0), (0, 0, 1, 3, 1),
         (7, 0, 1, 3, 1), (5, 0, 1, 3, 1), (1, 1, 0, 0, 0), (4, 1, 0, 0, 0), (0, 1, 3, 0, 0),
         (7, 1, 3, 0, 0), (0, 0, 3, 3, 1), (7, 0, 3, 3, 1), (5, 1, 3, 0, 0), (1, 1, 0, 1, 0),
         (4, 1, 0, 1, 0), (0, 1, 1, 0, 0), (7, 1, 1, 0, 0), (5, 1, 1, 0, 0), (0, 1, 3, 3, 0),
         (6, 1, 3, 3, 0), (7, 1, 3, 3, 0), (0, 0, 3, 1, 0), (7, 0, 3, 1, 0), (5, 1, 3, 3, 0),
         (0, 1, 3, 3, 1), (7, 1, 3, 3, 1), (0, 0, 1, 0, 1), (7, 0, 1, 0, 1), (0, 0, 2, 0, 0),
         (6, 0, 2, 0, 0), (5, 0, 2, 0, 0), (0, 0, 1, 1, 0), (7, 0, 1, 1, 0), (7, 0, 2, 0, 0),
         (0, 0, 3, 1, 1), (7, 0, 3, 1, 1),),
        ((0, 0, 2, 0, 1), (7, 0, 2, 0, 1), (5, 0, 2, 0, 1), (0, 0, 1, 1, 1), (7, 0, 1, 1, 1),
         (0, 1, 1, 2, 0), (6, 1, 1, 2, 0), (5, 1, 1, 2, 0), (7, 1, 1, 2, 0), (0, 0, 2, 3, 0),
         (6, 0, 2, 3, 0), (7, 0, 2, 3, 0), (0, 0, 1, 2, 1), (7, 0, 1, 2, 1),),
        ((0, 1, 1, 2, 1), (7, 1, 1, 2, 1), (1, 1, 0, 2, 0), (4, 1, 0, 2, 0), (0, 1, 1, 3, 0),
         (6, 1, 1, 3, 0), (7, 1, 1, 3, 0), (0, 0, 2, 1, 0), (7, 0, 2, 1, 0), (5, 0, 2, 1, 0),
         (6, 0, 2, 1, 0), (0, 0, 2, 3, 1), (7, 0, 2, 3, 1), (5, 0, 2, 3, 1), (0, 1, 3, 2, 1),
         (7, 1, 3, 2, 1), (6, 1, 3, 2, 1), (0, 1, 1, 3, 1), (7, 1, 1, 3, 1), (5, 1, 1, 2, 1),
         (0, 1, 1, 0, 1), (7, 1, 1, 0, 1), (0, 0, 2, 2, 0), (7, 0, 2, 2, 0), (5, 0, 2, 2, 0),
         (6, 0, 2, 2, 0), (0, 0, 2, 1, 1), (7, 0, 2, 1, 1), (5, 1, 1, 3, 0), (0, 1, 1, 1, 1),
         (7, 1, 1, 1, 1), (0, 1, 2, 2, 0), (7, 1, 2, 2, 0), (6, 1, 2, 2, 0), (0, 1, 3, 2, 0),
         (7, 1, 3, 2, 0), (5, 1, 1, 3, 1), (0, 1, 1, 1, 0), (7, 1, 1, 1, 0), (0, 1, 2, 1, 0),
         (6, 1, 2, 1, 0), (7, 1, 2, 1, 0), (0, 1, 2, 3, 0), (6, 1, 2, 3, 0), (7, 1, 2, 3, 0),
         (0, 0, 2, 2, 1), (7, 0, 2, 2, 1),),
        ((5, 1, 0, 1, 0),),
        ((0, 1, 3, 0, 1), (7, 1, 3, 0, 1), (0, 1, 2, 2, 1), (7, 1, 2, 2, 1), (5, 1, 0, 2, 0),
         (0, 1, 3, 1, 0), (7, 1, 3, 1, 0), (0, 1, 2, 1, 1), (7, 1, 2, 1, 1), (5, 1, 2, 2, 0),
         (0, 1, 2, 0, 0), (7, 1, 2, 0, 0), (0, 1, 2, 3, 1), (7, 1, 2, 3, 1), (5, 1, 2, 2, 1),
         (0, 1, 2, 0, 1), (7, 1, 2, 0, 1),),
        ((5, 1, 0, 3, 0), (0, 1, 3, 1, 1), (7, 1, 3, 1, 1),),
        (),
        ((5, 1, 0, 3, 1),),
    ),
    (
        ((3, 0, 0, 0, 0),),
        ((3, 0, 0, 1, 0),),
        (),
        (),
        (),
        (),
        (),
        (),
        (),
        (),
        (),
        ((3, 0, 0, 3, 0),),
        (),
        (),
        (),
        (),
        (),
        ((1, 0, 0, 0, 0), (4, 0, 0, 0, 0), (1, 0, 0, 1, 0), (4, 0, 0, 1, 0), (3, 0, 0, 2, 0),
         (1, 1, 0, 2, 0), (4, 1, 0, 2, 0), (3, 1, 0, 1, 0), (3, 1, 0, 2, 0), (3, 1, 0, 3, 0),),
        ((1, 1, 0, 1, 0), (4, 1, 0, 1, 0), (3, 1, 0, 0, 0),),
        (),
        (),
        (),
        (),
        (),
        (),
    ),
    (
        ((2, 0, 0, 0, 0),),
        (),
        ((3, 0, 0, 2, 0),),
        (),
        (),
        (),
        (),
        (),
        (),
        (),
        (),
        ((2, 0, 0, 1, 0),),
        (),
        (),
        (),
        (),
        ((3, 0, 0, 3, 0), (0, 0, 0, 0, 0), (6, 0, 0, 0, 0), (7, 0, 0, 0, 0), (2, 0, 0, 3, 0),
         (3, 1, 0, 2, 0), (0, 0, 0, 1, 0), (6, 0, 0, 1, 0), (7, 0, 0, 1, 0), (0, 0, 0, 0, 1),
         (7, 0, 0, 0, 1), (0, 0, 0, 2, 0), (6, 0, 0, 2, 0), (7, 0, 0, 2, 0), (0, 0, 0, 1, 1),
         (7, 0, 0, 1, 1), (2, 1, 0, 0, 0), (3, 1, 0, 3, 0), (0, 0, 1, 1, 0), (7, 0, 1, 1, 0),
         (6, 0, 1, 1, 0), (0, 0, 1, 0, 0), (6, 0, 1, 0, 0), (7, 0, 1, 0, 0), (0, 0, 0, 2, 1),
         (7, 0, 0, 2, 1), (0, 0, 0, 3, 0), (7, 0, 0, 3, 0), (6, 0, 0, 3, 0), (0, 0, 1, 1, 1),
         (7, 0, 1, 1, 1), (2, 1, 0, 1, 0), (0, 0, 1, 2, 0), (7, 0, 1, 2, 0), (6, 0, 1, 2, 0),
         (0, 0, 3, 0, 0), (7, 0, 3, 0, 0), (6, 0, 3, 0, 0), (0, 0, 1, 0, 1), (7, 0, 1, 0, 1),
         (0, 1, 1, 1, 0), (7, 1, 1, 1, 0), (0, 1, 0, 0, 1), (7, 1, 0, 0, 1), (0, 0, 0, 3, 1),
         (7, 0, 0, 3, 1),),
        ((5, 0, 1, 0, 1), (0, 0, 3, 2, 1), (7, 0, 3, 2, 1), (0, 0, 3, 1, 0), (5, 0, 3, 1, 0),
         (6, 0, 3, 1, 0), (7, 0, 3, 1, 0), (6, 0, 3, 2, 1), (0, 0, 1, 2, 1), (7, 0, 1, 2, 1),
         (0, 0, 3, 3, 0), (7, 0, 3, 3, 0), (6, 0, 3, 3, 0), (0, 0, 3, 0, 1), (7, 0, 3, 0, 1),
         (5, 0, 1, 1, 1), (0, 0, 1, 3, 1), (7, 0, 1, 3, 1), (6, 0, 1, 3, 1), (0, 0, 3, 1, 1),
         (7, 0, 3, 1, 1), (5, 0, 3, 1, 1), (5, 0, 1, 2, 1), (0, 1, 1, 0, 0), (7, 1, 1, 0, 0),
         (0, 0, 3, 2, 0), (7, 0, 3, 2, 0), (2, 1, 0, 2, 0), (0, 1, 3, 0, 0), (7, 1, 3, 0, 0),
         (0, 1, 3, 2, 0), (6, 1, 3, 2, 0), (7, 1, 3, 2, 0), (6, 1, 1, 0, 0), (0, 0, 3, 3, 1),
         (7, 0, 3, 3, 1),),
        ((0, 1, 2, 0, 0), (7, 1, 2, 0, 0), (0, 0, 2, 0, 0), (7, 0, 2, 0, 0), (6, 1, 1, 1, 0),
         (0, 0, 1, 3, 0), (7, 0, 1, 3, 0),),
        ((0, 1, 3, 3, 0), (7, 1, 3, 3, 0), (6, 1, 3, 0, 0), (0, 1, 3, 2, 1), (7, 1, 3, 2, 1),
         (5, 1, 3, 2, 1), (0, 1, 2, 1, 0), (7, 1, 2, 1, 0), (0, 0, 2, 0, 1), (7, 0, 2, 0, 1),
         (6, 1, 2, 0, 0), (0, 1, 1, 0, 1), (7, 1, 1, 0, 1), (5, 1, 1, 0, 1), (5, 1, 2, 1, 0),
         (0, 1, 1, 2, 0), (7, 1, 1, 2, 0), (0, 1, 1, 1, 1), (7, 1, 1, 1, 1), (5, 1, 1, 1, 1),
         (0, 0, 2, 1, 0), (7, 0, 2, 1, 0), (6, 0, 2, 1, 0), (0, 1, 3, 1, 0), (7, 1, 3, 1, 0),
         (0, 1, 3, 0, 1), (7, 1, 3, 0, 1), (5, 1, 3, 0, 1), (5, 1, 3, 1, 0), (0, 0, 2, 3, 1),
         (7, 0, 2, 3, 1), (6, 0, 2, 3, 1), (0, 1, 2, 0, 1), (7, 1, 2, 0, 1), (5, 1, 2, 0, 0),
         (0, 1, 2, 3, 0), (7, 1, 2, 3, 0), (0, 0, 2, 2, 0), (7, 0, 2, 2, 0), (6, 0, 2, 2, 0),
         (6, 1, 3, 1, 0), (0, 0, 2, 1, 1), (7, 0, 2, 1, 1), (5, 1, 2, 0, 1), (0, 1, 1, 2, 1),
         (7, 1, 1, 2, 1), (6, 1, 3, 3, 0), (0, 0, 2, 3, 0), (7, 0, 2, 3, 0), (0, 1, 1, 3, 0),
         (7, 1, 1, 3, 0), (6, 1, 2, 1, 0), (0, 0, 2, 2, 1), (7, 0, 2, 2, 1),),
        ((0, 1, 1, 3, 1), (7, 1, 1, 3, 1),),
        ((6, 1, 2, 3, 0), (0, 1, 3, 1, 1), (7, 1, 3, 1, 1), (5, 1, 3, 1, 1), (0, 1, 0, 1, 0),
         (7, 1, 0, 1, 0), (6, 1, 0, 0, 1), (0, 1, 3, 3, 1), (7, 1, 3, 3, 1),),
        ((0, 1, 0, 2, 0), (7, 1, 0, 2, 0), (6, 1, 0, 1, 0), (0, 1, 2, 1, 1), (7, 1, 2, 1, 1),
         (0, 1, 2, 2, 0), (7, 1, 2, 2, 0), (6, 1, 0, 2, 0), (0, 1, 2, 3, 1), (7, 1, 2, 3, 1),
         (0, 1, 2, 2, 1), (7, 1, 2, 2, 1),),
        ((0, 1, 0, 0, 0), (7, 1, 0, 0, 0), (0, 1, 0, 3, 0), (7, 1, 0, 3, 0), (0, 1, 0, 1, 1),
         (7, 1, 0, 1, 1), (0, 1, 0, 3, 1), (7, 1, 0, 3, 1), (0, 1, 0, 2, 1), (7, 1, 0, 2, 1),),
        (),
    ),
    (
        ((2, 0, 0, 0, 0), (3, 0, 0, 0, 0),),
        (),
        (),
        (),
        (),
        (),
        (),
        (),
        (),
        ((3, 0, 0, 2, 0),),
        (),
        ((2, 0, 0, 1, 0),),
        (),
        (),
        (),
        (),
        ((3, 0, 0, 3, 0), (2, 1, 0, 2, 0), (3, 1, 0, 0, 0), (2, 1, 0, 1, 0), (3, 1, 0, 3, 0),),
        (),
        (),
        (),
        (),
        (),
        (),
        (),
        (),
    ),
    (
        ((3, 0, 1, 0, 0),),
        ((2, 0, 1, 1, 0),),
        (),
        (),
        (),
        (),
        (),
        (),
        (),
        (),
        (),
        (),
        (),
        (),
        (),
        (),
        ((2, 1, 1, 1, 0), (3, 0, 1, 2, 0),),
        ((3, 0, 1, 3, 0), (1, 0, 1, 0, 0), (4, 0, 1, 0, 0), (3, 1, 1, 0, 0), (3, 0, 1, 1, 0),
         (3, 1, 1, 2, 0), (1, 0, 1, 3, 0), (4, 0, 1, 3, 0), (3, 1, 1, 3, 0), (1, 1, 1, 0, 0),
         (4, 1, 1, 0, 0), (3, 1, 1, 1, 0),),
        ((1, 1, 1, 1, 0), (4, 1, 1, 1, 0),),
        ((1, 1, 1, 2, 0), (4, 1, 1, 2, 0),),
        ((1, 0, 1, 2, 0), (4, 0, 1, 2, 0), (1, 1, 1, 3, 0), (4, 1, 1, 3, 0),),
        (),
        (),
        (),
        (),
    ),
    (
        ((5, 0, 1, 0, 0), (7, 0, 1, 0, 0),),
        (),
        (),
        (),
        (),
        ((7, 0, 1, 0, 1),),
        (),
        (),
        (),
        (),
        ((7, 0, 1, 1, 0),),
        (),
        (),
        (),
        (),
        ((7, 0, 1, 1, 1),),
        ((7, 0, 1, 2, 0), (7, 0, 1, 2, 1), (7, 0, 1, 3, 0), (7, 0, 1, 3, 1), (7, 1, 1, 0, 0),),
        ((7, 1, 1, 0, 1), (0, 0, 0, 0, 0), (5, 0, 0, 0, 0), (7, 0, 0, 0, 0), (7, 1, 1, 1, 0),
         (7, 1, 1, 1, 1), (7, 1, 1, 2, 0), (7, 1, 1, 2, 1), (7, 1, 1, 3, 0), (0, 0, 0, 1, 0),
         (5, 0, 0, 1, 0), (7, 0, 0, 1, 0), (1, 1, 1, 0, 0), (4, 1, 1, 0, 0), (7, 1, 1, 3, 1),
         (0, 0, 3, 2, 0), (6, 0, 3, 2, 0), (7, 0, 3, 2, 0), (0, 0, 0, 3, 0), (7, 0, 0, 3, 0),
         (5, 0, 0, 3, 0), (0, 0, 3, 2, 1), (7, 0, 3, 2, 1), (5, 0, 3, 2, 1), (0, 0, 3, 3, 0),
         (6, 0, 3, 3, 0), (7, 0, 3, 3, 0), (5, 0, 1, 1, 1), (5, 0, 1, 2, 0), (0, 0, 3, 3, 1),
         (7, 0, 3, 3, 1), (0, 1, 3, 2, 0), (6, 1, 3, 2, 0), (7, 1, 3, 2, 0), (5, 0, 1, 2, 1),
         (5, 0, 1, 3, 0), (0, 1, 3, 2, 1), (7, 1, 3, 2, 1), (0, 0, 3, 0, 0), (6, 0, 3, 0, 0),
         (7, 0, 3, 0, 0), (0, 1, 3, 3, 0), (7, 1, 3, 3, 0), (6, 1, 3, 3, 0), (5, 0, 1, 3, 1),
         (0, 0, 0, 2, 0), (7, 0, 0, 2, 0), (6, 0, 0, 2, 0), (0, 0, 3, 0, 1), (7, 0, 3, 0, 1),
         (5, 0, 0, 2, 0), (0, 0, 0, 0, 1), (7, 0, 0, 0, 1), (1, 1, 1, 1, 0), (4, 1, 1, 1, 0),
         (0, 1, 3, 3, 1), (7, 1, 3, 3, 1), (0, 0, 2, 1, 0), (7, 0, 2, 1, 0), (6, 0, 2, 1, 0),
         (0, 0, 0, 2, 1), (7, 0, 0, 2, 1), (5, 0, 0, 2, 1), (0, 0, 3, 1, 1), (6, 0, 3, 1, 1),
         (7, 0, 3, 1, 1), (1, 1, 1, 3, 0), (4, 1, 1, 3, 0), (0, 0, 2, 1, 1), (7, 0, 2, 1, 1),
         (5, 0, 2, 1, 1), (5, 1, 3, 3, 0), (0, 0, 2, 2, 0), (7, 0, 2, 2, 0), (6, 0, 2, 2, 0),
         (0, 1, 0, 1, 0), (7, 1, 0, 1, 0), (0, 0, 3, 1, 0), (7, 0, 3, 1, 0),),
        ((0, 1, 0, 2, 0), (7, 1, 0, 2, 0), (6, 1, 0, 2, 0), (0, 0, 0, 1, 1), (7, 0, 0, 1, 1),
         (0, 0, 2, 2, 1), (7, 0, 2, 2, 1), (5, 0, 2, 2, 1), (5, 1, 0, 1, 0), (0, 0, 2, 3, 0),
         (7, 0, 2, 3, 0), (6, 0, 2, 3, 0), (0, 0, 2, 0, 0), (6, 0, 2, 0, 0), (7, 0, 2, 0, 0),
         (0, 1, 0, 3, 0), (7, 1, 0, 3, 0), (6, 1, 0, 3, 0), (0, 1, 0, 2, 1), (7, 1, 0, 2, 1),
         (5, 1, 3, 2, 1), (0, 0, 0, 3, 1), (7, 0, 0, 3, 1),),
        ((0, 0, 2, 0, 1), (7, 0, 2, 0, 1), (5, 1, 0, 2, 1), (0, 1, 2, 3, 0), (7, 1, 2, 3, 0),
         (0, 1, 3, 0, 1), (6, 1, 3, 0, 1), (7, 1, 3, 0, 1), (0, 0, 2, 3, 1), (7, 0, 2, 3, 1),),
        ((0, 1, 0, 0, 0), (7, 1, 0, 0, 0), (0, 1, 3, 1, 1), (6, 1, 3, 1, 1), (7, 1, 3, 1, 1),
         (6, 1, 0, 0, 0), (0, 1, 0, 3, 1), (7, 1, 0, 3, 1), (5, 1, 0, 3, 1), (5, 1, 1, 0, 0),
         (0, 1, 3, 0, 0), (7, 1, 3, 0, 0), (0, 1, 2, 0, 0), (6, 1, 2, 0, 0), (7, 1, 2, 0, 0),
         (5, 1, 1, 1, 1), (0, 1, 3, 1, 0), (7, 1, 3, 1, 0),),
        ((5, 1, 1, 3, 0), (0, 1, 2, 1, 0), (7, 1, 2, 1, 0), (6, 1, 2, 1, 0), (6, 1, 2, 3, 0),
         (0, 1, 0, 0, 1), (7, 1, 0, 0, 1), (5, 1, 0, 0, 0), (0, 1, 0, 1, 1), (7, 1, 0, 1, 1),),
        ((0, 1, 2, 0, 1), (7, 1, 2, 0, 1), (5, 1, 0, 0, 1), (0, 1, 2, 2, 0), (7, 1, 2, 2, 0),
         (0, 1, 2, 1, 1), (7, 1, 2, 1, 1), (5, 1, 1, 2, 0), (0, 1, 2, 2, 1), (7, 1, 2, 2, 1),
         (0, 1, 2, 3, 1), (7, 1, 2, 3, 1),),
        ((5, 1, 1, 2, 1),),
        (),
    ),
    (
        ((2, 0, 1, 0, 0),),
        ((3, 0, 1, 1, 0),),
        (),
        ((2, 0, 1, 3, 0),),
        (),
        (),
        (),
        (),
        (),
        (),
        (),
        (),
        (),
        (),
        (),
        (),
        ((2, 1, 1, 0, 0), (1, 0, 1, 1, 0), (4, 0, 1, 1, 0), (2, 1, 1, 1, 0), (1, 1, 1, 1, 0),
         (4, 1, 1, 1, 0), (2, 1, 1, 2, 0), (2, 0, 1, 2, 0), (3, 0, 1, 2, 0), (2, 1, 1, 3, 0),
         (3, 0, 1, 3, 0),),
        ((3, 1, 1, 3, 0),),
        (),
        (),
        (),
        (),
        (),
        (),
        (),
    ),
    (
        ((3, 0, 1, 0, 0),),
        (),
        (),
        (),
        (),
        (),
        (),
        (),
        ((2, 1, 1, 0, 0),),
        (),
        (),
        (),
        (),
        (),
        (),
        (),
        ((2, 1, 1, 1, 0), (2, 1, 1, 3, 0), (0, 0, 1, 0, 0), (6, 0, 1, 0, 0), (7, 0, 1, 0, 0),
         (0, 0, 1, 0, 1), (7, 0, 1, 0, 1), (0, 0, 0, 0, 0), (6, 0, 0, 0, 0), (7, 0, 0, 0, 0),
         (0, 0, 3, 0, 0), (7, 0, 3, 0, 0), (6, 0, 3, 0, 0), (5, 0, 3, 0, 0), (0, 0, 0, 1, 0),
         (7, 0, 0, 1, 0), (6, 0, 0, 1, 0), (0, 0, 0, 0, 1), (7, 0, 0, 0, 1), (5, 0, 0, 0, 1),
         (0, 0, 3, 2, 1), (7, 0, 3, 2, 1), (6, 0, 3, 2, 1), (0, 0, 3, 0, 1), (7, 0, 3, 0, 1),
         (0, 0, 3, 1, 0), (7, 0, 3, 1, 0), (6, 0, 3, 1, 0), (0, 0, 0, 3, 0), (7, 0, 0, 3, 0),
         (0, 0, 0, 1, 1), (7, 0, 0, 1, 1), (0, 0, 1, 1, 1), (7, 0, 1, 1, 1), (6, 0, 0, 3, 0),
         (0, 0, 3, 1, 1), (7, 0, 3, 1, 1), (5, 0, 3, 1, 1), (0, 0, 3, 3, 0), (7, 0, 3, 3, 0),
         (6, 0, 3, 3, 0), (3, 0, 1, 3, 0), (0, 0, 1, 2, 0), (7, 0, 1, 2, 0), (6, 0, 1, 1, 1),
         (0, 0, 3, 2, 0), (7, 0, 3, 2, 0), (5, 0, 0, 1, 1), (0, 0, 1, 2, 1), (7, 0, 1, 2, 1),
         (0, 0, 3, 3, 1), (7, 0, 3, 3, 1),),
        ((0, 1, 3, 0, 0), (7, 1, 3, 0, 0), (6, 1, 3, 0, 0), (3, 0, 1, 1, 0), (0, 0, 1, 3, 0),
         (7, 0, 1, 3, 0), (0, 0, 0, 3, 1), (7, 0, 0, 3, 1), (0, 0, 2, 0, 0), (7, 0, 2, 0, 0),
         (5, 0, 2, 0, 0), (0, 0, 1, 3, 1), (7, 0, 1, 3, 1), (6, 0, 2, 0, 0), (0, 0, 1, 1, 0),
         (7, 0, 1, 1, 0),),
        ((0, 1, 3, 1, 0), (7, 1, 3, 1, 0), (6, 1, 3, 1, 0), (3, 0, 1, 2, 0), (5, 0, 0, 3, 1),
         (0, 0, 0, 2, 0), (7, 0, 0, 2, 0), (0, 1, 3, 0, 1), (7, 1, 3, 0, 1), (5, 1, 3, 0, 1),
         (0, 0, 0, 2, 1), (7, 0, 0, 2, 1),),
        ((0, 0, 2, 3, 0), (6, 0, 2, 3, 0), (7, 0, 2, 3, 0), (0, 1, 3, 1, 1), (7, 1, 3, 1, 1),
         (3, 1, 1, 2, 0), (5, 1, 3, 1, 1), (0, 0, 2, 1, 1), (7, 0, 2, 1, 1), (6, 0, 2, 1, 1),
         (0, 0, 2, 0, 1), (7, 0, 2, 0, 1), (3, 1, 1, 3, 0), (0, 1, 3, 3, 0), (7, 1, 3, 3, 0),
         (6, 1, 3, 3, 0), (0, 0, 2, 3, 1), (7, 0, 2, 3, 1), (0, 0, 2, 2, 1), (7, 0, 2, 2, 1),
         (0, 0, 2, 1, 0), (7, 0, 2, 1, 0), (0, 1, 3, 2, 0), (7, 1, 3, 2, 0), (0, 1, 0, 1, 0),
         (6, 1, 0, 1, 0), (7, 1, 0, 1, 0), (0, 1, 2, 0, 0), (5, 1, 2, 0, 0), (6, 1, 2, 0, 0),
         (7, 1, 2, 0, 0), (0, 1, 3, 3, 1), (7, 1, 3, 3, 1), (0, 1, 3, 2, 1), (7, 1, 3, 2, 1),
         (0, 1, 2, 1, 0), (5, 1, 2, 1, 0), (7, 1, 2, 1, 0), (6, 1, 2, 1, 0), (0, 1, 0, 1, 1),
         (5, 1, 0, 1, 1), (7, 1, 0, 1, 1), (0, 1, 0, 2, 1), (7, 1, 0, 2, 1), (6, 1, 0, 2, 1),
         (0, 1, 2, 2, 0), (7, 1, 2, 2, 0), (6, 1, 2, 2, 0), (5, 1, 2, 2, 0), (0, 1, 2, 0, 1),
         (7, 1, 2, 0, 1), (0, 1, 0, 3, 1), (7, 1, 0, 3, 1), (0, 0, 2, 2, 0), (7, 0, 2, 2, 0),),
        ((0, 1, 2, 1, 1), (7, 1, 2, 1, 1),),
        ((0, 1, 1, 0, 0), (7, 1, 1, 0, 0), (6, 1, 0, 3, 1), (0, 1, 2, 3, 0), (7, 1, 2, 3, 0),
         (6, 1, 2, 3, 0), (0, 1, 2, 2, 1), (5, 1, 2, 2, 1), (7, 1, 2, 2, 1), (0, 1, 1, 1, 1),
         (7, 1, 1, 1, 1), (6, 1, 1, 0, 0), (0, 1, 0, 2, 0), (7, 1, 0, 2, 0), (0, 1, 1, 3, 0),
         (7, 1, 1, 3, 0), (6, 1, 1, 1, 1), (0, 1, 2, 3, 1), (7, 1, 2, 3, 1),),
        ((0, 1, 0, 0, 0), (7, 1, 0, 0, 0), (6, 1, 1, 3, 0), (0, 1, 0, 3, 0), (7, 1, 0, 3, 0),
         (0, 1, 0, 0, 1), (7, 1, 0, 0, 1),),
        ((0, 1, 1, 0, 1), (7, 1, 1, 0, 1), (0, 1, 1, 2, 0), (7, 1, 1, 2, 0), (0, 1, 1, 1, 0),
         (7, 1, 1, 1, 0), (0, 1, 1, 2, 1), (7, 1, 1, 2, 1), (0, 1, 1, 3, 1), (7, 1, 1, 3, 1),),
        (),
    ),
)


def local_plain(tokens, norm_gain, up_trained, down_trained):
    shards = lax.axis_size("fs")
    groups = lax.axis_size("tp")
    rows_local = up_trained.shape[0]
    cols_local = up_trained.shape[1]
    folded = (norm_gain[:, None] * up_trained).astype(jnp.bfloat16)
    stacked = jnp.stack([folded, down_trained.astype(jnp.bfloat16)])
    served_width = cols_local * groups // shards
    blocks_here = cols_local // served_width
    quarter_rows = rows_local // groups
    pieces = stacked.reshape(2, groups, quarter_rows, blocks_here, served_width)
    moved = lax.all_to_all(pieces, "tp", split_axis=1, concat_axis=3, tiled=True)
    placed = lax.all_to_all(moved, "fs", split_axis=3, concat_axis=2, tiled=True)
    ordered = placed.reshape(2, shards, quarter_rows, served_width)
    joined = lax.all_gather(ordered, "tp", axis=2, tiled=True)
    owned = joined.reshape(2, rows_local * shards, served_width)
    up_serving = owned[0]
    down_serving = owned[1]
    values = tokens.astype(jnp.float32)
    scale = lax.rsqrt(jnp.mean(values * values, axis=1, keepdims=True) + epsilon)
    normed = (values * scale).astype(jnp.bfloat16)
    hidden = jnp.dot(normed, up_serving, preferred_element_type=jnp.float32)
    active = jnp.square(jax.nn.relu(hidden)).astype(jnp.bfloat16)
    summed = lax.psum_scatter(
        lax.dot_general(
            down_serving, active, (((1,), (1,)), ((), ())), preferred_element_type=jnp.float32
        ),
        "fs",
        scatter_dimension=0,
        tiled=True,
    )
    prompt_output = summed.T.astype(jnp.bfloat16)
    return (up_serving, down_serving, prompt_output)


def down_block(active, whole, plane, put):
    rows_local = whole.shape[1] // 4
    tile = 256 if rows_local % 256 == 0 else rows_local

    @pl.loop(0, rows_local // tile)
    def _(n):
        rows = pl.ds(pl.multiple_of(plane * rows_local + n * tile, tile), tile)
        product = lax.dot_general(
            active[...], whole[1, rows, :], (((1,), (1,)), ((), ())),
            preferred_element_type=jnp.float32,
        )
        put(pl.ds(pl.multiple_of(n * tile, tile), tile), product)


def kernel(
    tokens_hbm, gain_hbm, up_hbm, down_hbm, whole, active, rs_recv,
    raw, gain_rows, gain, cast, relay, toks, normed, hidden, rs_send,
    in_sem, misc_sem, got_sem, relay_sem, block_sem, src_sem, out_sem, rs_ssem, rs_rsem,
):
    y = lax.axis_index("grp")
    z = lax.axis_index("fs")
    t = lax.axis_index("tp")
    mirrored = z // 2
    role = jnp.where(mirrored == 1, 4 * (3 - z) + (3 - t), 4 * z + t)
    is_own = z == t
    is_active = t % 2 == z % 2
    t_x = jnp.where(t < 2, t + 2, t - 2)
    t_c = t + 1 - 2 * (t % 2)
    to_x = {"tp": t_x}
    to_c = {"tp": t_c}
    to_y = {"grp": 1 - y}
    rows_local, width = cast.shape[1], cast.shape[2]
    size = rows_local // (2 * PAIRS)
    trained = (up_hbm, down_hbm)
    planes = [jnp.where(mirrored == 1, 3 - k, k) for k in range(4)]
    sides = [y, 1 - y]

    def part(pair, side):
        return 2 * pair + sides[side]

    def ds(start, extent):
        return pl.ds(pl.multiple_of(start, extent), extent)

    def local_rows(pair, side):
        return ds(part(pair, side) * size, size)

    def unit(m, plane, pair, side):
        return whole.at[m, ds(plane * rows_local + part(pair, side) * size, size)]

    def remote(src, dst, ssem, rsem, where):
        return pltpu.make_async_remote_copy(
            src_ref=src, dst_ref=dst, send_sem=ssem, recv_sem=rsem,
            device_id=where, device_id_type=MESH,
        )

    def fetch(m, pair, side):
        rows = local_rows(pair, side)
        return pltpu.make_async_copy(
            trained[m].at[rows], raw.at[m, rows], in_sem.at[m, 2 * pair + side]
        )

    get_gain = pltpu.make_async_copy(gain_hbm, gain_rows, misc_sem.at[0])
    get_toks = pltpu.make_async_copy(tokens_hbm, toks, misc_sem.at[1])
    get_gain.start()
    for pair in range(PAIRS):
        fetch(0, pair, 0).start()

    barrier = pltpu.get_barrier_semaphore()
    others = [{"fs": lax.rem(z + k, 4)} for k in range(1, 4)]
    for where in [to_x, to_c, to_y] + others:
        pl.semaphore_signal(barrier, inc=1, device_id=where, device_id_type=MESH)

    get_gain.wait()
    lanes = gain_rows.shape[1]
    for q in range(gain_rows.shape[0]):
        square = (lanes, lanes)
        chosen = jnp.where(
            lax.broadcasted_iota(jnp.int32, square, 0) == lax.broadcasted_iota(jnp.int32, square, 1),
            jnp.broadcast_to(gain_rows[pl.ds(q, 1), :], square), 0.0,
        )
        column = jnp.sum(chosen, axis=1, keepdims=True)
        gain[pl.ds(q * lanes, lanes), :] = jnp.broadcast_to(column, square)

    piece = 16

    def cast_unit(m, pair, side):
        fetch(m, pair, side).wait()
        base = part(pair, side) * size

        def store(into, shift):
            @pl.loop(0, size // piece)
            def _(i):
                here = ds(base + i * piece, piece)
                there = ds(shift + base + i * piece, piece)
                if m == 0:
                    factor = gain[here, :]
                    for j in range(width // lanes):
                        cols = pl.ds(j * lanes, lanes)
                        into[0, there, cols] = (raw[0, here, cols] * factor).astype(jnp.bfloat16)
                else:
                    into[m, there, :] = raw[m, here, :].astype(jnp.bfloat16)

        @pl.when(is_own)
        def _():
            store(whole, z * rows_local)

        if side == 0:
            @pl.when(jnp.logical_not(is_own))
            def _():
                store(cast, 0)

    def step(kind, m, k, pair, side):
        plane = planes[k]
        place = part(pair, side)
        if kind == GET:
            here = unit(m, plane, pair, side)
            remote(here, here, out_sem.at[0, m], got_sem.at[m, plane, place], to_x).wait_recv()
        elif kind == GET_RELAY:
            here = relay.at[m, ds(place * size, size)]
            remote(here, here, src_sem.at[m], relay_sem.at[m, place], to_x).wait_recv()
        elif kind == SWAP:
            remote(
                cast.at[m, local_rows(pair, side)], relay.at[m, ds(place * size, size)],
                src_sem.at[m], relay_sem.at[m, place], to_x,
            ).start()
        elif kind in (HOP, HOP_RELAY):
            src = (cast if kind == HOP else relay).at[m, ds(place * size, size)]
            remote(
                src, unit(m, z, pair, side), src_sem.at[m], got_sem.at[m, z, place],
                {"fs": t if kind == HOP else t_x},
            ).start()
        elif kind == SEND_CORE:
            here = unit(m, plane, pair, side)
            remote(here, here, out_sem.at[2, m], block_sem.at[m, plane], to_c).start()
        else:
            here = unit(m, plane, pair, side)
            i = kind - SEND_X
            remote(
                here, here, out_sem.at[i, m], got_sem.at[m, plane, place], (to_x, to_y)[i]
            ).start()

    def run(segment):
        for r in range(8):
            if SCHEDULE[r][segment]:
                @pl.when(role == r)
                def _():
                    for s in SCHEDULE[r][segment]:
                        step(*s)

    casts = [(m, pair, side) for m in range(2) for side in range(2) for pair in range(PAIRS)]
    segment = 0
    for m, pair, side in casts:
        if side == 1:
            pl.when(is_own)(lambda: cast_unit(m, pair, side))
        else:
            cast_unit(m, pair, side)
        if segment == 0:
            @pl.when(is_own)
            def _():
                for p in range(PAIRS):
                    fetch(0, p, 1).start()
            for p in range(PAIRS):
                fetch(1, p, 0).start()
            @pl.when(is_own)
            def _():
                for p in range(PAIRS):
                    fetch(1, p, 1).start()
            get_toks.start()
            pl.semaphore_wait(barrier, 6)
        run(segment)
        segment += 1

    get_toks.wait()
    tokens_here = toks.shape[0]

    @pl.loop(0, tokens_here // piece)
    def _(i):
        here = ds(i * piece, piece)
        values = toks[here, :].astype(jnp.float32)
        scale = lax.rsqrt(jnp.mean(values * values, axis=1, keepdims=True) + epsilon)
        normed[here, :] = (values * scale).astype(jnp.bfloat16)

    def pick(table):
        chosen = planes[table[0]]
        for r in range(1, 8):
            if table[r] != table[0]:
                chosen = jnp.where(role == r, planes[table[r]], chosen)
        return chosen

    def listen(m, plane):
        @pl.when(jnp.logical_not(is_active))
        def _():
            here = whole.at[m, ds(plane * rows_local, rows_local)]
            remote(here, here, out_sem.at[2, m], block_sem.at[m, plane], to_c).wait_recv()

    tile = 512 if width % 512 == 0 else width

    def compute_up(k):
        plane = pick(ORDER[0][k])
        listen(0, plane)
        rows = ds(plane * rows_local, rows_local)

        @pl.loop(0, width // tile)
        def _(n):
            cols = ds(n * tile, tile)
            product = jnp.dot(
                normed[:, rows], whole[0, rows, cols], preferred_element_type=jnp.float32
            )
            if k > 0:
                product = product + hidden[:, cols]
            if k < 3:
                hidden[:, cols] = product
            else:
                active[:, cols] = jnp.square(jnp.maximum(product, 0.0)).astype(jnp.bfloat16)

    def scatter(k, plane):
        slot = lax.rem(z - plane + 3, 4)
        return remote(
            rs_send.at[k], rs_recv.at[slot], rs_ssem.at[k], rs_rsem.at[slot], {"fs": plane}
        )

    def compute_down(k):
        plane = pick(ORDER[1][k])
        listen(1, plane)

        down_block(
            active, whole, plane,
            lambda cols, product: rs_send.__setitem__((k, slice(None), cols), product.astype(jnp.bfloat16)),
        )
        scatter(k, plane).start()

    for m in range(2):
        for k in range(4):
            run(segment)
            segment += 1
            if m == 0:
                compute_up(k)
            elif k < 3:
                compute_down(k)
            else:
                listen(1, z)
    run(segment)

    for k in range(3):
        here = rs_recv.at[k]
        remote(here, here, rs_ssem.at[k], rs_rsem.at[k], {"fs": lax.rem(z + 1, 4)}).wait_recv()

    def drain(sem, m, count):
        sent = whole.at[m, pl.ds(0, count * size)]
        remote(sent, sent, sem, got_sem.at[0, 0, 0], to_x).wait_send()

    for r in range(8):
        @pl.when(role == r)
        def _():
            for m in range(2):
                steps = [s for part_of in SCHEDULE[r] for s in part_of if s[1] == m]
                hops = sum(s[0] in (SWAP, HOP, HOP_RELAY) for s in steps)
                if hops:
                    drain(src_sem.at[m], m, hops)
                for i, kind in enumerate((SEND_X, SEND_Y, SEND_CORE)):
                    sends = sum(s[0] == kind for s in steps)
                    if sends:
                        drain(out_sem.at[i, m], m, sends)
    for k in range(3):
        here = rs_send.at[k]
        remote(here, here, rs_ssem.at[k], rs_rsem.at[k], {"fs": lax.rem(z + 1, 4)}).wait_send()


pieces_out = 8


def deliver(whole, active, rs_recv, up_out, down_out, prompt_out, own, prompt, sems, last):
    rows = whole.shape[1] // pieces_out
    copies = [
        pltpu.make_async_copy(
            whole.at[m, pl.ds(i * rows, rows)], out.at[pl.ds(i * rows, rows)], sems.at[m, i]
        )
        for m, out in enumerate((up_out, down_out))
        for i in range(pieces_out)
    ]
    for copy in copies:
        copy.start()
    down_block(
        active, whole, lax.axis_index("fs"),
        lambda cols, product: own.__setitem__((slice(None), cols), product),
    )
    piece = 16

    @pl.loop(0, own.shape[0] // piece)
    def _(i):
        here = pl.ds(pl.multiple_of(i * piece, piece), piece)
        total = own[here, :]
        for k in range(3):
            total = total + rs_recv[k, here, :].astype(jnp.float32)
        prompt[here, :] = total.astype(prompt.dtype)

    copies.append(pltpu.make_async_copy(prompt, prompt_out, last))
    copies[-1].start()
    for copy in copies:
        copy.wait()


def local_kernel(tokens, norm_gain, up_trained, down_trained):
    shards = lax.axis_size("fs")
    rows_local, width = up_trained.shape
    tokens_here, features = tokens.shape
    any_space = pl.BlockSpec(memory_space=pl.ANY)
    dma = pltpu.SemaphoreType.DMA
    bf16, f32 = jnp.bfloat16, jnp.float32
    results = pl.pallas_call(
        kernel,
        out_shape=(
            pltpu.VMEM((2, rows_local * shards, width), bf16),
            pltpu.VMEM((tokens_here, width), bf16),
            pltpu.VMEM((3, tokens_here, rows_local), bf16),
        ),
        in_specs=[any_space] * 4,
        out_specs=(pl.BlockSpec(memory_space=pltpu.VMEM),) * 3,
        scratch_shapes=[
            pltpu.VMEM((2, rows_local, width), f32),
            pltpu.VMEM((rows_local // 128, 128), f32),
            pltpu.VMEM((rows_local, 128), f32),
            pltpu.VMEM((2, rows_local, width), bf16),
            pltpu.VMEM((2, rows_local, width), bf16),
            pltpu.VMEM((tokens_here, features), bf16),
            pltpu.VMEM((tokens_here, features), bf16),
            pltpu.VMEM((tokens_here, width), f32),
            pltpu.VMEM((3, tokens_here, rows_local), bf16),
            dma((2, 2 * PAIRS)), dma((2,)),
            dma((2, 4, 2 * PAIRS)), dma((2, 2 * PAIRS)), dma((2, 4)),
            dma((2,)), dma((3, 2)), dma((3,)), dma((3,)),
        ],
        compiler_params=pltpu.CompilerParams(
            collective_id=0, has_side_effects=True, vmem_limit_bytes=40 * 1024 * 1024
        ),
    )(tokens, norm_gain.reshape(rows_local // 128, 128), up_trained, down_trained)
    held = pl.BlockSpec(memory_space=pltpu.VMEM)
    return tuple(pl.pallas_call(
        deliver,
        out_shape=(
            jax.ShapeDtypeStruct((rows_local * shards, width), bf16),
            jax.ShapeDtypeStruct((rows_local * shards, width), bf16),
            jax.ShapeDtypeStruct((tokens_here, rows_local), bf16),
        ),
        in_specs=[held] * 3,
        out_specs=(any_space,) * 3,
        scratch_shapes=[
            pltpu.VMEM((tokens_here, rows_local), f32), pltpu.VMEM((tokens_here, rows_local), bf16),
            dma((2, pieces_out)), dma(()),
        ],
        compiler_params=pltpu.CompilerParams(vmem_limit_bytes=8 * 1024 * 1024),
    )(*results))


def solution(mesh):
    in_specs = (P(("grp", "tp"), None), P("fs"), P("fs", "tp"), P("fs", "tp"))
    out_specs = (P("grp", "fs"), P("grp", "fs"), P(("grp", "tp"), "fs"))
    sizes = mesh.shape
    square = sizes["grp"] == 2 and sizes["fs"] == 4 and sizes["tp"] == 4
    local = local_kernel if square else local_plain
    return jax.shard_map(local, mesh=mesh, in_specs=in_specs, out_specs=out_specs, check_vma=False)
```

time: 99.4 us -> 98.3 us (0.989)
  no operation moved by 1% of the time
where the time goes in v4:
time: 98.3 us; the launch traced here: 98.1 us
  Pallas kernels  97.5 us (99%)
    pallas_call x1, Pallas kernels, local_kernel(): pl.pallas_call(kernel, out_shape=(pltpu.VMEM((2, rows_local * shards, wid...  91.5 us
    pallas_call x1, Pallas kernels, local_kernel(): pl.pallas_call(deliver, out_shape=(jax.ShapeDtypeStruct((rows_local * sha...  5.99 us

profile of v4, /device:TPU:3, one launch (start us, length us, event | category | flops | bytes accessed | tf_op | source)
XLA Modules:
  0.0 98.1 jit_solution(7737100437091742631)
XLA Ops:
  0.6 91.5 %shard_map.67 = (bf16[2,2048,2048]{2,1,0:T(8,128)(2,1)S(1)}, bf16[192,2048]{1,0:T(8,128)(2,1)S(1)}, bf16[3,192,512]{2,1,0:T(8,128)(2,1)S(1)}) custom-call(bf16[192,2048]{1,0:T(8,128)(2,1)} %tokens_hbm.1, f32[4,128]{1,0:T(4,128)} %bitcast.1, f32[512,2048]{1,0:T(8,128)} %up_hbm.1, f32[512,2048]{1,0:T(8,128)} %down_hbm.1), custom_call_target="tpu_custom_call" | custom-call | tf_op jit(solution)/shard_map/pallas_call | solution.py:711
  92.1 6.0 %shard_map.68 = (bf16[2048,2048]{1,0:T(8,128)(2,1)}, bf16[2048,2048]{1,0:T(8,128)(2,1)}, bf16[192,512]{1,0:T(8,128)(2,1)}) custom-call(bf16[2,2048,2048]{2,1,0:T(8,128)(2,1)S(1)} %get-tuple-element.6.whole, bf16[192,2048]{1,0:T(8,128)(2,1)S(1)} %get-tuple-element.7.active, bf16[3,192,512]{2,1,0:T(8,128)(2,1)S(1)} %get-tuple-element.8.rs_recv), custom_call_target="tpu_custom_call" | custom-call | tf_op jit(solution)/shard_map/pallas_call | solution.py:739

commit v5 on v4

--- a/solution.py
+++ b/solution.py
@@ -416,7 +416,7 @@
 def kernel(
     tokens_hbm, gain_hbm, up_hbm, down_hbm, whole, active, rs_recv,
     raw, gain_rows, gain, cast, relay, toks, normed, hidden, rs_send,
-    in_sem, misc_sem, got_sem, relay_sem, block_sem, src_sem, out_sem, rs_ssem, rs_rsem,
+    in_sem, misc_sem, got_sem, relay_sem, src_sem, out_sem, rs_ssem, rs_rsem,
 ):
     y = lax.axis_index("grp")
     z = lax.axis_index("fs")
@@ -518,11 +518,11 @@
             remote(here, here, out_sem.at[0, m], got_sem.at[m, plane, place], to_x).wait_recv()
         elif kind == GET_RELAY:
             here = relay.at[m, ds(place * size, size)]
-            remote(here, here, src_sem.at[m], relay_sem.at[m, place], to_x).wait_recv()
+            remote(here, here, src_sem.at[m], relay_sem.at[m, pair], to_x).wait_recv()
         elif kind == SWAP:
             remote(
                 cast.at[m, local_rows(pair, side)], relay.at[m, ds(place * size, size)],
-                src_sem.at[m], relay_sem.at[m, place], to_x,
+                src_sem.at[m], relay_sem.at[m, pair], to_x,
             ).start()
         elif kind in (HOP, HOP_RELAY):
             src = (cast if kind == HOP else relay).at[m, ds(place * size, size)]
@@ -532,7 +532,7 @@
             ).start()
         elif kind == SEND_CORE:
             here = unit(m, plane, pair, side)
-            remote(here, here, out_sem.at[2, m], block_sem.at[m, plane], to_c).start()
+            remote(here, here, out_sem.at[2, m], got_sem.at[m, plane, 0], to_c).start()
         else:
             here = unit(m, plane, pair, side)
             i = kind - SEND_X
@@ -592,7 +592,7 @@
         @pl.when(jnp.logical_not(is_active))
         def _():
             here = whole.at[m, ds(plane * rows_local, rows_local)]
-            remote(here, here, out_sem.at[2, m], block_sem.at[m, plane], to_c).wait_recv()
+            remote(here, here, out_sem.at[2, m], got_sem.at[m, plane, 0], to_c).wait_recv()
 
     tile = 512 if width % 512 == 0 else width
 
@@ -674,7 +674,7 @@
     rows = whole.shape[1] // pieces_out
     copies = [
         pltpu.make_async_copy(
-            whole.at[m, pl.ds(i * rows, rows)], out.at[pl.ds(i * rows, rows)], sems.at[m, i]
+            whole.at[m, pl.ds(i * rows, rows)], out.at[pl.ds(i * rows, rows)], sems.at[m]
         )
         for m, out in enumerate((up_out, down_out))
         for i in range(pieces_out)
@@ -695,10 +695,11 @@
             total = total + rs_recv[k, here, :].astype(jnp.float32)
         prompt[here, :] = total.astype(prompt.dtype)
 
-    copies.append(pltpu.make_async_copy(prompt, prompt_out, last))
-    copies[-1].start()
-    for copy in copies:
-        copy.wait()
+    final = pltpu.make_async_copy(prompt, prompt_out, last)
+    final.start()
+    for m, out in enumerate((up_out, down_out)):
+        pltpu.make_async_copy(whole.at[m], out, sems.at[m]).wait()
+    final.wait()
 
 
 def local_kernel(tokens, norm_gain, up_trained, down_trained):
@@ -728,7 +729,7 @@
             pltpu.VMEM((tokens_here, width), f32),
             pltpu.VMEM((3, tokens_here, rows_local), bf16),
             dma((2, 2 * PAIRS)), dma((2,)),
-            dma((2, 4, 2 * PAIRS)), dma((2, 2 * PAIRS)), dma((2, 4)),
+            dma((2, 4, 2 * PAIRS)), dma((2, PAIRS)),
             dma((2,)), dma((3, 2)), dma((3,)), dma((3,)),
         ],
         compiler_params=pltpu.CompilerParams(
@@ -747,7 +748,7 @@
         out_specs=(any_space,) * 3,
         scratch_shapes=[
             pltpu.VMEM((tokens_here, rows_local), f32), pltpu.VMEM((tokens_here, rows_local), bf16),
-            dma((2, pieces_out)), dma(()),
+            dma((2,)), dma(()),
         ],
         compiler_params=pltpu.CompilerParams(vmem_limit_bytes=8 * 1024 * 1024),
     )(*results))

time: 98.3 us -> 98 us (level)
  no operation moved by 1% of the time
where the time goes in v5:
time: 98 us; the launch traced here: 97.9 us
  Pallas kernels  97.2 us (99%)
    pallas_call x1, Pallas kernels, local_kernel(): pl.pallas_call(kernel, out_shape=(pltpu.VMEM((2, rows_local * shards, wid...  91.3 us
    pallas_call x1, Pallas kernels, local_kernel(): pl.pallas_call(deliver, out_shape=(jax.ShapeDtypeStruct((rows_local * sha...  5.87 us

profile of v5, /device:TPU:3, one launch (start us, length us, event | category | flops | bytes accessed | tf_op | source)
XLA Modules:
  0.0 97.9 jit_solution(7374542327108254903)
XLA Ops:
  0.6 91.3 %shard_map.67 = (bf16[2,2048,2048]{2,1,0:T(8,128)(2,1)S(1)}, bf16[192,2048]{1,0:T(8,128)(2,1)S(1)}, bf16[3,192,512]{2,1,0:T(8,128)(2,1)S(1)}) custom-call(bf16[192,2048]{1,0:T(8,128)(2,1)} %tokens_hbm.1, f32[4,128]{1,0:T(4,128)} %bitcast.1, f32[512,2048]{1,0:T(8,128)} %up_hbm.1, f32[512,2048]{1,0:T(8,128)} %down_hbm.1), custom_call_target="tpu_custom_call" | custom-call | tf_op jit(solution)/shard_map/pallas_call | solution.py:712
  92.0 5.9 %shard_map.68 = (bf16[2048,2048]{1,0:T(8,128)(2,1)}, bf16[2048,2048]{1,0:T(8,128)(2,1)}, bf16[192,512]{1,0:T(8,128)(2,1)}) custom-call(bf16[2,2048,2048]{2,1,0:T(8,128)(2,1)S(1)} %get-tuple-element.6.whole, bf16[192,2048]{1,0:T(8,128)(2,1)S(1)} %get-tuple-element.7.active, bf16[3,192,512]{2,1,0:T(8,128)(2,1)S(1)} %get-tuple-element.8.rs_recv), custom_call_target="tpu_custom_call" | custom-call | tf_op jit(solution)/shard_map/pallas_call | solution.py:740

commit v6 on v5

--- a/solution.py
+++ b/solution.py
@@ -482,7 +482,18 @@
         column = jnp.sum(chosen, axis=1, keepdims=True)
         gain[pl.ds(q * lanes, lanes), :] = jnp.broadcast_to(column, square)
 
+    tokens_here = toks.shape[0]
     piece = 16
+
+    def norm():
+        get_toks.wait()
+
+        @pl.loop(0, tokens_here // piece)
+        def _(i):
+            here = ds(i * piece, piece)
+            values = toks[here, :].astype(jnp.float32)
+            scale = lax.rsqrt(jnp.mean(values * values, axis=1, keepdims=True) + epsilon)
+            normed[here, :] = (values * scale).astype(jnp.bfloat16)
 
     def cast_unit(m, pair, side):
         fetch(m, pair, side).wait()
@@ -567,19 +578,12 @@
                 for p in range(PAIRS):
                     fetch(1, p, 1).start()
             get_toks.start()
+            pl.when(z == 0)(norm)
             pl.semaphore_wait(barrier, 6)
         run(segment)
         segment += 1
 
-    get_toks.wait()
-    tokens_here = toks.shape[0]
-
-    @pl.loop(0, tokens_here // piece)
-    def _(i):
-        here = ds(i * piece, piece)
-        values = toks[here, :].astype(jnp.float32)
-        scale = lax.rsqrt(jnp.mean(values * values, axis=1, keepdims=True) + epsilon)
-        normed[here, :] = (values * scale).astype(jnp.bfloat16)
+    pl.when(z != 0)(norm)
 
     def pick(table):
         chosen = planes[table[0]]

time: 98 us -> 99.9 us (1.019)
  Pallas kernels: 97.2 us -> 99.1 us
    pallas_call x1, Pallas kernels: 91.3 us -> 93.2 us  [local_kernel(): pl.pallas_call(kernel, out_shape=(pltpu.VMEM((2, rows_local * shards, wid...]
where the time goes in v6:
time: 99.9 us; the launch traced here: 99.7 us
  Pallas kernels  99.1 us (99%)
    pallas_call x1, Pallas kernels, local_kernel(): pl.pallas_call(kernel, out_shape=(pltpu.VMEM((2, rows_local * shards, wid...  93.2 us
    pallas_call x1, Pallas kernels, local_kernel(): pl.pallas_call(deliver, out_shape=(jax.ShapeDtypeStruct((rows_local * sha...  5.87 us

profile of v6, /device:TPU:3, one launch (start us, length us, event | category | flops | bytes accessed | tf_op | source)
XLA Modules:
  0.0 99.7 jit_solution(16921687999514925073)
XLA Ops:
  0.6 93.2 %shard_map.67 = (bf16[2,2048,2048]{2,1,0:T(8,128)(2,1)S(1)}, bf16[192,2048]{1,0:T(8,128)(2,1)S(1)}, bf16[3,192,512]{2,1,0:T(8,128)(2,1)S(1)}) custom-call(bf16[192,2048]{1,0:T(8,128)(2,1)} %tokens_hbm.1, f32[4,128]{1,0:T(4,128)} %bitcast.1, f32[512,2048]{1,0:T(8,128)} %up_hbm.1, f32[512,2048]{1,0:T(8,128)} %down_hbm.1), custom_call_target="tpu_custom_call" | custom-call | tf_op jit(solution)/shard_map/pallas_call | solution.py:716
  93.8 5.9 %shard_map.68 = (bf16[2048,2048]{1,0:T(8,128)(2,1)}, bf16[2048,2048]{1,0:T(8,128)(2,1)}, bf16[192,512]{1,0:T(8,128)(2,1)}) custom-call(bf16[2,2048,2048]{2,1,0:T(8,128)(2,1)S(1)} %get-tuple-element.6.whole, bf16[192,2048]{1,0:T(8,128)(2,1)S(1)} %get-tuple-element.7.active, bf16[3,192,512]{2,1,0:T(8,128)(2,1)S(1)} %get-tuple-element.8.rs_recv), custom_call_target="tpu_custom_call" | custom-call | tf_op jit(solution)/shard_map/pallas_call | solution.py:744
